TPU v7x, 32 devices: a whole 2x2x4 slice. The times are simulated.
32 devices in a mesh: sp: 4 (over z), fs: 4 (over y, x), tp: 2 (over core).
Axes of the slice: x: 2, y: 2, z: 4, core: 2. Of those that a mesh axis runs over, the one named last changes fastest.
Arguments:
- tokens: bfloat16 [12288, 2048], P(('fs', 'sp'), 'tp'), parts along dimension 0, may hold values from -6 to 6
- norm_gain: bfloat16 [2048], replicated, may hold values from 0.099609375 to 1.8984375
- w_query: bfloat16 [2048, 1024], P(None, 'tp'), may hold values from -0.125 to 0.125
- w_key: bfloat16 [2048, 1024], P(None, 'tp'), may hold values from -0.125 to 0.125
- w_value: bfloat16 [2048, 1024], P(None, 'tp'), may hold values from -0.125 to 0.125
- log_decay: float32 [8, 3072], P('tp', 'sp'), may hold values from -1 to 0
- w_conv_in: bfloat16 [2048, 1024], P(None, 'tp'), may hold values from -0.125 to 0.125
- w_conv_pre: bfloat16 [2048, 1024], P(None, 'tp'), may hold values from -0.125 to 0.125
- w_conv_post: bfloat16 [2048, 1024], P(None, 'tp'), may hold values from -0.125 to 0.125
- conv_taps: bfloat16 [3, 1024], P(None, 'tp'), may hold values from -3 to 3
- w_out_ret: bfloat16 [1024, 2048], replicated, may hold values from -0.125 to 0.125
- w_out_conv: bfloat16 [1024, 2048], replicated, may hold values from -0.125 to 0.125
Outputs:
- mixed: bfloat16 [12288, 2048], P(('fs', 'sp', 'tp')), parts along dimension 0
There are 4 independent parts, one for each index of `fs`. A program takes and returns all parts, laid end to end along the dimension named above; an argument that names none is the same for every part. Nothing has to cross between parts.
All inputs are finite; a program needn't handle non-finite values.
Results may differ from a plain program's by a relative error of at most 0.012.
Values may be sent and summed in bfloat16 or wider, within the bound.
No kernel may reach another device: no remote copies, remote signals or barrier semaphores. Data moves between devices by JAX's collectives and lax.ppermute only.
A program may use at most 128 MiB of HBM per device.

v0:
```python
import jax
import jax.numpy as jnp
from jax import lax
from jax.sharding import PartitionSpec as P

DH = 128
TAPS = 3
SPAN = 128


epsilon = 1e-06


def shifted(value, axis, steps):
    count = lax.axis_size(axis)
    first, last = (max(0, -steps), min(count, count - steps))
    return lax.ppermute(value, axis, [(source, source + steps) for source in range(first, last)])


def rotate(vectors, positions):
    halfway = vectors.shape[-1] // 2
    inverse = 10000.0 ** (-jnp.arange(halfway, dtype=jnp.float32) / halfway)
    angles = positions.astype(jnp.float32)[:, None] * inverse[None, :]
    cosines = jnp.cos(angles)[:, None, :]
    sinusoid = jnp.sin(angles)[:, None, :]
    leading = vectors[..., :halfway]
    trailing = vectors[..., halfway:]
    return jnp.concatenate(
        [leading * cosines - trailing * sinusoid, leading * sinusoid + trailing * cosines], axis=-1
    )


def body(
    tokens,
    norm_gain,
    w_query,
    w_key,
    w_value,
    log_decay,
    w_conv_in,
    w_conv_pre,
    w_conv_post,
    conv_taps,
    w_out_ret,
    w_out_conv,
):
    gathered = lax.all_gather(tokens, "tp", axis=1, tiled=True)
    floats = gathered.astype(jnp.float32)
    normed = (
        floats
        * lax.rsqrt(jnp.mean(floats * floats, axis=-1, keepdims=True) + epsilon)
        * norm_gain.astype(jnp.float32)
    ).astype(jnp.bfloat16)
    tok_rows = normed.shape[0]
    head_count = w_query.shape[1] // DH
    positions = lax.axis_index("sp") * tok_rows + jnp.arange(tok_rows, dtype=jnp.int32)

    def project(weight):
        return jnp.dot(normed, weight, preferred_element_type=jnp.float32)

    queries = rotate(project(w_query).reshape(tok_rows, head_count, DH), positions).astype(
        jnp.bfloat16
    )
    keys_turned = (
        rotate(project(w_key).reshape(tok_rows, head_count, DH), positions) * DH ** (-0.5)
    ).astype(jnp.bfloat16)
    values = project(w_value).astype(jnp.bfloat16).reshape(tok_rows, head_count, DH)
    conv_in = lax.optimization_barrier(project(w_conv_in).astype(jnp.bfloat16))
    conv_pre = lax.optimization_barrier(project(w_conv_pre).astype(jnp.bfloat16))
    conv_post = lax.optimization_barrier(project(w_conv_post).astype(jnp.bfloat16))
    gated_in = (conv_pre.astype(jnp.float32) * conv_in.astype(jnp.float32)).astype(jnp.bfloat16)
    rim_rows = shifted(gated_in[tok_rows - (TAPS - 1) :], "sp", 1)
    extended = jnp.concatenate([rim_rows, gated_in], axis=0)
    convolved = jnp.zeros(gated_in.shape, jnp.float32)
    for tap_index in range(TAPS):
        convolved = convolved + conv_taps[tap_index].astype(jnp.float32) * extended[
            tap_index : tap_index + tok_rows
        ].astype(jnp.float32)
    conv_out = (conv_post.astype(jnp.float32) * convolved).astype(jnp.bfloat16)
    blocks = tok_rows // SPAN
    query_blocks = queries.reshape(blocks, SPAN, head_count, DH)
    key_blocks = keys_turned.reshape(blocks, SPAN, head_count, DH)
    value_blocks = values.reshape(blocks, SPAN, head_count, DH)
    cumulative = jnp.cumsum(log_decay.reshape(head_count, blocks, SPAN), axis=-1).transpose(1, 0, 2)
    lower_mask = jnp.tril(jnp.ones((SPAN, SPAN), bool))
    differences = cumulative[..., :, None] - cumulative[..., None, :]
    decay_weights = jnp.where(lower_mask, jnp.exp(jnp.minimum(differences, 0.0)), 0.0)
    scores = jnp.einsum(
        "bshd,bthd->bhst", query_blocks, key_blocks, preferred_element_type=jnp.float32
    )
    mix_weights = (scores * decay_weights).astype(jnp.bfloat16)
    inside = jnp.einsum(
        "bhst,bthd->bshd", mix_weights, value_blocks, preferred_element_type=jnp.float32
    )
    block_ends = cumulative[..., -1]
    tail_decay = jnp.exp(block_ends[..., None] - cumulative)
    weighted = value_blocks.astype(jnp.float32) * tail_decay.transpose(0, 2, 1)[..., None]
    block_states = jnp.einsum(
        "bshd,bshe->bhde", key_blocks.astype(jnp.float32), weighted, precision=lax.Precision.HIGHEST
    )

    def advance(carried, inputs):
        end_decay, fresh_state = inputs
        return (jnp.exp(end_decay)[:, None, None] * carried + fresh_state, carried)

    empty_state = jnp.zeros((head_count, DH, DH), jnp.float32)
    local_total, local_starts = lax.scan(advance, empty_state, (block_ends, block_states))
    decay_total = jnp.exp(jnp.sum(block_ends, axis=0))
    all_decays, all_states = (
        lax.all_gather(decay_total[None].astype(jnp.bfloat16), "sp", axis=0, tiled=True).astype(
            jnp.float32
        ),
        lax.all_gather(local_total[None].astype(jnp.bfloat16), "sp", axis=0, tiled=True).astype(
            jnp.float32
        ),
    )
    position_index = lax.axis_index("sp")

    def absorb(source, carried):
        absorbed = all_decays[source][:, None, None] * carried + all_states[source]
        return jnp.where(source < position_index, absorbed, carried)

    incoming = lax.fori_loop(0, lax.axis_size("sp"), absorb, empty_state)
    prefix_ends = jnp.cumsum(block_ends, axis=0) - block_ends
    starts = local_starts + jnp.exp(prefix_ends)[..., None, None] * incoming[None]
    across = jnp.einsum(
        "bshd,bhde->bshe", query_blocks.astype(jnp.float32), starts, precision=lax.Precision.HIGHEST
    )
    retained = inside + jnp.exp(cumulative).transpose(0, 2, 1)[..., None] * across
    normalized = retained * lax.rsqrt(
        jnp.mean(retained * retained, axis=-1, keepdims=True) + epsilon
    )
    ret_out = normalized.astype(jnp.bfloat16).reshape(tok_rows, head_count * DH)
    ret_width = ret_out.shape[1]
    conv_width = conv_out.shape[1]
    pair_index = lax.axis_index("tp")
    ret_rows = lax.dynamic_slice_in_dim(w_out_ret, pair_index * ret_width, ret_width, 0)
    conv_rows = lax.dynamic_slice_in_dim(w_out_conv, pair_index * conv_width, conv_width, 0)
    return lax.psum_scatter(
        (
            jnp.dot(ret_out, ret_rows, preferred_element_type=jnp.float32)
            + jnp.dot(conv_out, conv_rows, preferred_element_type=jnp.float32)
        ).astype(jnp.bfloat16),
        "tp",
        scatter_dimension=0,
        tiled=True,
    )


def solution(mesh):
    in_specs = (
        P(("fs", "sp"), "tp"),
        P(),
        P(None, "tp"),
        P(None, "tp"),
        P(None, "tp"),
        P("tp", "sp"),
        P(None, "tp"),
        P(None, "tp"),
        P(None, "tp"),
        P(None, "tp"),
        P(),
        P(),
    )
    out_specs = P(("fs", "sp", "tp"), None)
    return jax.shard_map(body, mesh=mesh, in_specs=in_specs, out_specs=out_specs, check_vma=False)
```

profile of v0, /device:TPU:0, one launch (start us, length us, event | category | flops | bytes accessed | tf_op | source)
XLA Modules:
  0.0 141.2 jit_solution(10205250472383561693)
XLA Ops:
  7.3 0.7 reshape.136
  8.0 1.2 dynamic-slice
  9.9 1.1 reduce_window_sum.22
  11.5 13.5 %all-reduce = bf16[16]{0:T(256)(128)(2,1)S(1)} all-reduce(bf16[16]{0:T(256)(128)(2,1)S(1)} %dynamic-update-slice), channel_id=2, replica_groups=mesh['sp'=4,'fs'=4,'tp'=2] {'sp'}, use_global_device_ids=true, to_apply=%add | all-reduce | flops 16 | bytes 64
  26.3 0.8 slice_convert_fusion.2
  27.1 1.5 %multiply_cosine_fusion = (f32[768,64]{0,1:T(8,128)}, f32[768,64]{0,1:T(8,128)}) fusion(f32[64]{0:T(128)S(1)} %multiply_power_fusion, f32[768]{0:T(1024)S(1)} %add_convert_fusion.2), kind=kLoop, calls=%fused_computation.62 | loop fusion | flops 49152 | bytes 396544 | tf_op jit(solution)/shard_map/cos | solution.py:24
  28.6 2.7 %fusion.3 = f32[768]{0:T(1024)S(1)} fusion(bf16[768,2048]{1,0:T(8,128)(2,1)} %all-gather.4.cloned.1.call-done), kind=kLoop, calls=%fused_computation.10 | loop fusion | flops 4717824 | bytes 3148800 | tf_op jit(solution)/shard_map/reduce_sum | solution.py:51
  31.4 1.8 %convolution_convert_fusion.1 = bf16[768,512]{1,0:T(8,128)(2,1)S(1)} fusion(bf16[2048,512]{1,0:T(8,128)(2,1)S(1)} %copy-done, bf16[768,2048]{1,0:T(8,128)(2,1)S(1)} %copy-done.1, f32[2048]{0:T(1024)S(1)} %convert_element_type.106, f32[768]{0:T(1024)S(1)} %add_rsqrt_fusion.1), kind=kOutput, calls=%fused_computation.33 | convolution fusion | flops 1617297408 | bytes 6040576 | tf_op jit(solution)/shard_map/dot_general | solution.py:59
  33.3 1.8 %convolution_convert_fusion = bf16[768,512]{1,0:T(8,128)(2,1)S(1)} fusion(bf16[2048,512]{1,0:T(8,128)(2,1)S(1)} %copy-done.12, bf16[768,2048]{1,0:T(8,128)(2,1)S(1)} %copy-done.1, f32[2048]{0:T(1024)S(1)} %convert_element_type.106, f32[768]{0:T(1024)S(1)} %add_rsqrt_fusion.1), kind=kOutput, calls=%fused_computation.32 | convolution fusion | flops 1617297408 | bytes 6040576 | tf_op jit(solution)/shard_map/dot_general | solution.py:59
  35.4 0.9 copy-done.7
  36.3 1.5 %collective-permute-start = (bf16[2,512]{1,0:T(2,128)(2,1)S(1)}, bf16[2,512]{1,0:T(2,128)(2,1)S(1)}, u32[]{:S(2)}, u32[]{:S(2)}) collective-permute-start(bf16[2,512]{1,0:T(2,128)(2,1)S(1)} %slice.49), channel_id=1, source_target_pairs={{0,8},{8,16},{16,24},{1,9},{9,17},{17,25},{2,10},{10,18},{18,26},{... | collective-permute-start | bytes 6152 | tf_op jit(solution)/shard_map/ppermute | solution.py:17
  37.8 2.7 %convolution_convert_fusion.3 = bf16[768,512]{1,0:T(8,128)(2,1)} fusion(bf16[2048,512]{1,0:T(8,128)(2,1)S(1)} %copy-done.13, bf16[768,2048]{1,0:T(8,128)(2,1)S(1)} %copy-done.1, f32[2048]{0:T(1024)S(1)} %convert_element_type.106, f32[768]{0:T(1024)S(1)} %add_rsqrt_fusion.1), kind=kOutput, calls=%fused_computation.35 | convolution fusion | flops 1617297408 | bytes 6040576 | tf_op jit(solution)/shard_map/dot_general | solution.py:59
  40.5 1.7 %reshape_reshape.3 = bf16[6,128,4,128]{3,2,1,0:T(4,128)(2,1)S(1)} reshape(bf16[768,512]{1,0:T(8,128)(2,1)} %convolution_convert_fusion.3) | data formatting | bytes 1572864 | tf_op jit(solution)/shard_map/reshape;reshape | solution.py:83
  42.3 4.9 %fusion.49 = f32[768,512]{0,1:T(8,128)S(1)} fusion(bf16[2048,512]{1,0:T(8,128)(2,1)} %param.18, bf16[768,2048]{1,0:T(8,128)(2,1)} %all-gather.4.cloned.1.call-done, f32[2048]{0:T(1024)S(1)} %convert_element_type.106, f32[768]{0:T(1024)S(1)} %add_rsqrt_fusion.1), kind=kOutput, calls=%fused_computation.85 | convolution fusion | flops 1616904192 | bytes 6827008 | tf_op jit(solution)/shard_map/dot_general | solution.py:59
  47.2 2.0 %fusion.47 = f32[768,512]{0,1:T(8,128)S(1)} fusion(bf16[2048,512]{1,0:T(8,128)(2,1)S(1)} %copy-done.14, bf16[768,2048]{1,0:T(8,128)(2,1)S(1)} %copy-done.2, f32[2048]{0:T(1024)S(1)} %convert_element_type.106, f32[768]{0:T(1024)S(1)} %add_rsqrt_fusion.1), kind=kOutput, calls=%fused_computation.84 | convolution fusion | flops 1616904192 | bytes 6827008 | tf_op jit(solution)/shard_map/dot_general | solution.py:59
  49.2 1.7 %subtract_convert_fusion = (bf16[768,4,64]{0,2,1:T(8,128)(2,1)}, bf16[768,4,64]{0,2,1:T(8,128)(2,1)}, f32[768,4,64]{0,2,1:T(8,128)}, f32[768,4,64]{0,2,1:T(8,128)}) fusion(f32[768,4,128]{0,2,1:T(8,128)S(1)} %bitcast.70, f32[768,64]{0,1:T(8,128)S(1)} %copy-done.10, f32[768,64]{0,1:T(8,128)S(1)} %copy-done.9, f32[768,4,128]{0,2,1:T(8,128)S(1)} %bitcast.71), kind=kLoop, calls=%fused_computation.57 | loop fusion | flops 2752512 | bytes 5898240 | tf_op jit(solution)/shard_map/convert.6
  51.0 2.3 %concatenate.20 = bf16[6,128,4,64]{1,0,3,2:T(8,128)(2,1)} reshape(bf16[768,4,64]{0,2,1:T(8,128)(2,1)} %get-tuple-element.203) | data formatting | bytes 786432 | tf_op jit(solution)/shard_map/concatenate | solution.py:28
  53.2 2.3 %copy.36 = bf16[6,128,4,64]{3,1,2,0:T(8,128)(2,1)} copy(bf16[6,128,4,64]{1,0,3,2:T(8,128)(2,1)} %concatenate.20) | data formatting | bytes 786432 | tf_op jit(solution)/shard_map/concatenate | solution.py:28
  55.5 2.2 %concatenate.21 = bf16[6,128,4,64]{1,0,3,2:T(8,128)(2,1)} reshape(bf16[768,4,64]{0,2,1:T(8,128)(2,1)} %get-tuple-element.204) | data formatting | bytes 786432 | tf_op jit(solution)/shard_map/concatenate | solution.py:28
  57.8 2.3 %copy.37 = bf16[6,128,4,64]{3,1,2,0:T(8,128)(2,1)} copy(bf16[6,128,4,64]{1,0,3,2:T(8,128)(2,1)} %concatenate.21) | data formatting | bytes 786432 | tf_op jit(solution)/shard_map/concatenate | solution.py:28
  60.1 2.3 %concatenate.24 = f32[6,128,4,64]{1,0,3,2:T(8,128)} reshape(f32[768,4,64]{0,2,1:T(8,128)} %get-tuple-element.207) | data formatting | bytes 1572864 | tf_op jit(solution)/shard_map/concatenate | solution.py:28
  62.3 2.9 %copy.39 = f32[6,128,4,64]{3,1,2,0:T(8,128)} copy(f32[6,128,4,64]{1,0,3,2:T(8,128)} %concatenate.24) | data formatting | bytes 1572864 | tf_op jit(solution)/shard_map/concatenate | solution.py:28
  65.2 2.3 %concatenate.23 = f32[6,128,4,64]{1,0,3,2:T(8,128)} reshape(f32[768,4,64]{0,2,1:T(8,128)} %get-tuple-element.208) | data formatting | bytes 1572864 | tf_op jit(solution)/shard_map/concatenate | solution.py:28
  67.5 2.9 %copy.38 = f32[6,128,4,64]{3,1,2,0:T(8,128)} copy(f32[6,128,4,64]{1,0,3,2:T(8,128)} %concatenate.23) | data formatting | bytes 1572864 | tf_op jit(solution)/shard_map/concatenate | solution.py:28
  70.3 2.4 %fusion.9 = bf16[6,128,4,128]{3,1,2,0:T(8,128)(2,1)S(1)} fusion(f32[6,128,4,64]{3,1,2,0:T(8,128)} %copy.39, f32[6,128,4,64]{3,1,2,0:T(8,128)} %copy.38), kind=kLoop, calls=%fused_computation.18 | loop fusion | flops 1179648 | bytes 2359296 | tf_op jit(solution)/shard_map/convert_element_type | solution.py:66
  72.7 2.6 %fusion.14 = f32[6,4,128,128]{3,2,1,0:T(8,128)} fusion(bf16[6,128,4,128]{3,1,2,0:T(8,128)(2,1)S(1)} %fusion.9, f32[6,128,4]{1,2,0:T(4,128)S(1)} %copy.45, bf16[6,128,4,128]{3,2,1,0:T(4,128)(2,1)S(1)} %reshape_reshape.3), kind=kOutput, calls=%fused_computation.28 | convolution fusion | flops 604766208 | bytes 3158016 | tf_op jit(solution)/shard_map/bshd,bshe->bhde/dot_general | solution.py:98
  75.3 10.8 %while.29 = (s32[]{:T(128)}, f32[4,128,128]{2,1,0:T(8,128)S(1)}, f32[6,4,128,128]{3,2,1,0:T(8,128)}, f32[6,4]{1,0:T(8,128)S(1)}, f32[6,4,128,128]{3,2,1,0:T(8,128)}) while((s32[]{:T(128)}, f32[4,128,128]{2,1,0:T(8,128)S(1)}, f32[6,4,128,128]{3,2,1,0:T(8,128)}, f32[6,4]{1,0:T(8,128)S(1)}, ...), condition=%wide.region_3.4_spmd.clone.clone, body=%wide.region_2.3_spmd.clone.sunk.clone | while | flops 262147 | bytes 1310860 | solution.py:107
  75.3 0.7 bitcast_dynamic-update-slice_fusion.3
  76.0 1.0 bitcast_add_fusion.4
  77.1 0.7 bitcast_dynamic-update-slice_fusion.3
  77.9 1.0 bitcast_add_fusion.4
  78.9 0.7 bitcast_dynamic-update-slice_fusion.3
  79.7 1.0 bitcast_add_fusion.4
  80.7 0.7 bitcast_dynamic-update-slice_fusion.3
  81.5 1.0 bitcast_add_fusion.4
  82.5 0.7 bitcast_dynamic-update-slice_fusion.3
  83.3 1.0 bitcast_add_fusion.4
  84.3 0.7 bitcast_dynamic-update-slice_fusion.3
  85.1 1.0 bitcast_add_fusion.4
  86.2 15.6 %all-gather.1 = bf16[16,128,128]{2,1,0:T(8,128)(2,1)S(1)} all-gather(bf16[4,128,128]{2,1,0:T(8,128)(2,1)S(1)} %convert_element_type.116), channel_id=3, replica_groups=mesh['sp'=4,'fs'=4,'tp'=2] {'sp'}, dimensions={0}, use_global_device_ids=true | all-gather | bytes 655360 | tf_op jit(solution)/shard_map/all_gather | solution.py:113
  102.4 4.3 %fusion.19 = f32[6,4,128,128]{3,2,1,0:T(8,128)} fusion(bf16[6,128,4,128]{3,1,2,0:T(8,128)(2,1)} %copy-done.5, f32[6,4,128]{2,1,0:T(4,128)S(1)} %copy.40, pred[128,128]{1,0:T(8,128)(4,1)S(1)} %iota_compare_fusion, bf16[6,128,4,128]{3,2,1,0:T(4,128)(2,1)} %copy-done.3, bf16[6,128,4,64]{3,1,2,0:T(8,128)(2,1)} %copy.37, bf16[6,128,4,64]{3,1,2,0:T(8,128)(2,1)} %copy.36), kind=kOutput, calls=%fused_computation.36 | convolution fusion | flops 204865536 | bytes 3960832 | tf_op jit(solution)/shard_map/bhst,bthd->bshd/dot_general | solution.py:92
  106.8 3.9 %multiply_reduce_fusion = (f32[6,128,4]{1,2,0:T(4,128)S(1)}, f32[6,128,4,128]{1,3,2,0:T(8,128)S(1)}) fusion(bf16[6,128,4,64]{3,1,2,0:T(8,128)(2,1)} %copy.37, bf16[6,128,4,64]{3,1,2,0:T(8,128)(2,1)S(1)} %copy-done.4, f32[6,4,128,128]{3,2,1,0:T(8,128)} %get-tuple-element.127, f32[4,128,128]{2,1,0:T(8,128)S(1)} %get-tuple-element.129, f32[6,4]{1,0:T(8,128)S(1)} %copy.48, ...), kind=kOutput, calls=%fused_computation.24 | convolution fusion | flops 607908864 | bytes 5791840 | tf_op jit(solution)/shard_map/bshd,bhde->bshe/dot_general | solution.py:126
  110.7 1.1 multiply_convert_fusion.2
  111.8 1.5 %copy.50 = bf16[6,128,4,128]{3,2,1,0:T(4,128)(2,1)S(1)} copy(bf16[6,128,4,128]{1,3,2,0:T(8,128)(2,1)} %multiply_convert_fusion.2) | data formatting | bytes 1572864 | tf_op jit(solution)/shard_map/convert_element_type | solution.py:133
  113.3 4.5 %convolution_convert_fusion.2 = bf16[768,512]{1,0:T(8,128)(2,1)S(1)} fusion(bf16[2048,512]{1,0:T(8,128)(2,1)} %param.24, bf16[768,2048]{1,0:T(8,128)(2,1)} %all-gather.4.cloned.1.call-done, f32[2048]{0:T(1024)S(1)} %convert_element_type.106, f32[768]{0:T(1024)S(1)} %add_rsqrt_fusion.1), kind=kOutput, calls=%fused_computation.34 | convolution fusion | flops 1617297408 | bytes 6040576 | tf_op jit(solution)/shard_map/dot_general | solution.py:59
  117.9 1.8 %fusion.7 = f32[768,2048]{1,0:T(8,128)S(1)} fusion(bf16[1024,2048]{1,0:T(8,128)(2,1)S(1)} %copy-done.6, s32[]{:T(128)S(6)} %select_n.33, bf16[96,8,4,128]{3,2,1,0:T(4,128)(2,1)S(1)} %bitcast.68), kind=kOutput, calls=%fused_computation.15 | convolution fusion | flops 1610612736 | bytes 9175044 | tf_op jit(solution)/shard_map/dot_general | solution.py:141
  120.3 3.8 %add_convert_fusion = bf16[768,2048]{1,0:T(8,128)(2,1)} fusion(f32[768,2048]{1,0:T(8,128)S(1)} %fusion.7, bf16[1024,2048]{1,0:T(8,128)(2,1)S(1)} %copy-done.11, s32[]{:T(128)S(6)} %select_n.33, bf16[768,512]{1,0:T(8,128)(2,1)S(1)} %copy-done.8, bf16[768,512]{1,0:T(8,128)(2,1)S(1)} %convolution_convert_fusion.2, ...), kind=kOutput, calls=%fused_computation.13 | convolution fusion | flops 1620443136 | bytes 13115396 | tf_op jit(solution)/shard_map/dot_general | solution.py:142
  124.2 10.2 %reduce-scatter.2.cloned.1.call-done = bf16[384,2048]{1,0:T(8,128)(2,1)} async-done(((bf16[768,2048]{1,0:T(8,128)(2,1)}), bf16[384,2048]{1,0:T(8,128)(2,1)}) %reduce-scatter.2.cloned.1.call-update) | async-done | bytes 1572880 | tf_op jit(solution)/shard_map/reduce_scatter | solution.py:139
  (76 shorter events, 4.6 us)
Async XLA Ops:
  6.5 24.8 %copy-start = (bf16[2048,512]{1,0:T(8,128)(2,1)S(1)}, bf16[2048,512]{1,0:T(8,128)(2,1)}, u32[]{:S(2)}) copy-start(bf16[2048,512]{1,0:T(8,128)(2,1)} %param.23) | copy-start | bytes 6291460
  6.5 22.1 %all-gather.4.cloned.1.call-start = ((), (), s32[]{:S(2)}) async-start(), calls=%async_computation.1 | async-start | bytes 4718592 | tf_op jit(solution)/shard_map/all_gather | solution.py:47
  7.3 127.1 %reduce-scatter.2.cloned.1.call-start = ((), (), s32[]{:S(2)}) async-start(), calls=%async_computation.2 | async-start | bytes 4718592 | tf_op jit(solution)/shard_map/reduce_scatter | solution.py:139
  28.6 2.8 %copy-start.1 = (bf16[768,2048]{1,0:T(8,128)(2,1)S(1)}, bf16[768,2048]{1,0:T(8,128)(2,1)}, u32[]{:S(2)}) copy-start(bf16[768,2048]{1,0:T(8,128)(2,1)} %all-gather.4.cloned.1.call-done) | copy-start | bytes 9437188
  31.4 1.9 %copy-start.12 = (bf16[2048,512]{1,0:T(8,128)(2,1)S(1)}, bf16[2048,512]{1,0:T(8,128)(2,1)}, u32[]{:S(2)}) copy-start(bf16[2048,512]{1,0:T(8,128)(2,1)} %param.22) | copy-start | bytes 6291460
  35.2 2.6 %copy-start.13 = (bf16[2048,512]{1,0:T(8,128)(2,1)S(1)}, bf16[2048,512]{1,0:T(8,128)(2,1)}, u32[]{:S(2)}) copy-start(bf16[2048,512]{1,0:T(8,128)(2,1)} %param.20) | copy-start | bytes 6291460
  35.4 0.9 copy-start.7
  36.3 83.4 %collective-permute-start = (bf16[2,512]{1,0:T(2,128)(2,1)S(1)}, bf16[2,512]{1,0:T(2,128)(2,1)S(1)}, u32[]{:S(2)}, u32[]{:S(2)}) collective-permute-start(bf16[2,512]{1,0:T(2,128)(2,1)S(1)} %slice.49), channel_id=1, source_target_pairs={{0,8},{8,16},{16,24},{1,9},{9,17},{17,25},{2,10},{10,18},{18,26},{... | collective-permute-start | bytes 6152 | tf_op jit(solution)/shard_map/ppermute | solution.py:17
  42.2 30.4 %copy-start.3 = (bf16[6,128,4,128]{3,2,1,0:T(4,128)(2,1)}, bf16[6,128,4,128]{3,2,1,0:T(4,128)(2,1)S(1)}, u32[]{:S(2)}) copy-start(bf16[6,128,4,128]{3,2,1,0:T(4,128)(2,1)S(1)} %reshape_reshape.3) | copy-start | bytes 2359300
  42.2 4.9 %copy-start.2 = (bf16[768,2048]{1,0:T(8,128)(2,1)S(1)}, bf16[768,2048]{1,0:T(8,128)(2,1)}, u32[]{:S(2)}) copy-start(bf16[768,2048]{1,0:T(8,128)(2,1)} %all-gather.4.cloned.1.call-done) | copy-start | bytes 9437188
  42.3 4.9 %copy-start.14 = (bf16[2048,512]{1,0:T(8,128)(2,1)S(1)}, bf16[2048,512]{1,0:T(8,128)(2,1)}, u32[]{:S(2)}) copy-start(bf16[2048,512]{1,0:T(8,128)(2,1)} %param.19) | copy-start | bytes 6291460
  47.2 2.1 %copy-start.9 = (f32[768,64]{0,1:T(8,128)S(1)}, f32[768,64]{0,1:T(8,128)}, u32[]{:S(2)}) copy-start(f32[768,64]{0,1:T(8,128)} %get-tuple-element.211) | copy-start | bytes 589828
  47.2 2.1 %copy-start.10 = (f32[768,64]{0,1:T(8,128)S(1)}, f32[768,64]{0,1:T(8,128)}, u32[]{:S(2)}) copy-start(f32[768,64]{0,1:T(8,128)} %get-tuple-element.212) | copy-start | bytes 589828
  72.7 2.6 %copy-start.5 = (bf16[6,128,4,128]{3,1,2,0:T(8,128)(2,1)}, bf16[6,128,4,128]{3,1,2,0:T(8,128)(2,1)S(1)}, u32[]{:S(2)}) copy-start(bf16[6,128,4,128]{3,1,2,0:T(8,128)(2,1)S(1)} %fusion.9) | copy-start | bytes 2359300
  102.4 4.3 %copy-start.4 = (bf16[6,128,4,64]{3,1,2,0:T(8,128)(2,1)S(1)}, bf16[6,128,4,64]{3,1,2,0:T(8,128)(2,1)}, u32[]{:S(2)}) copy-start(bf16[6,128,4,64]{3,1,2,0:T(8,128)(2,1)} %copy.36) | copy-start | bytes 1179652
  113.3 4.6 %copy-start.6 = (bf16[1024,2048]{1,0:T(8,128)(2,1)S(1)}, bf16[1024,2048]{1,0:T(8,128)(2,1)}, u32[]{:S(2)}) copy-start(bf16[1024,2048]{1,0:T(8,128)(2,1)} %param.26) | copy-start | bytes 12582916
  117.9 1.9 %copy-start.8 = (bf16[768,512]{1,0:T(8,128)(2,1)S(1)}, bf16[768,512]{1,0:T(8,128)(2,1)}, u32[]{:S(2)}) copy-start(bf16[768,512]{1,0:T(8,128)(2,1)} %copy-done.7) | copy-start | bytes 2359300
  117.9 2.4 %copy-start.11 = (bf16[1024,2048]{1,0:T(8,128)(2,1)S(1)}, bf16[1024,2048]{1,0:T(8,128)(2,1)}, u32[]{:S(2)}) copy-start(bf16[1024,2048]{1,0:T(8,128)(2,1)} %param.27) | copy-start | bytes 12582916
Sparse Core Ops, SparseCore 0:
  8.9 14.8 all-gather.3
  124.3 10.0 reduce-scatter.1
where the time goes:
time: 142 us; the launch traced here: 141 us
  matrix products  34.4 us (24%)
  blocking collectives  29 us (20%)
  local copies, waits for them, and re-layouts  26.8 us (19%)
  other arithmetic  23.9 us (17%)
  between operations  14.4 us (10%)
  waiting for transfers between devices  10.9 us (8%)
  starting transfers between devices  1.5 us (1%)
    concatenate x8, local copies, waits for them, and re-layouts, rotate(): jnp.concatenate([leading * cosines - trailing * sinusoid, leading * sinus...  19.3 us
    dot_general x6, matrix products, project(): return jnp.dot(normed, weight, preferred_element_type=jnp.float32)  17.8 us
    all_gather x1, blocking collectives, body(): lax.all_gather(local_total[None].astype(jnp.bfloat16), 'sp', axis=0, tile...  15.6 us
    unnamed x1, blocking collectives  13.5 us
    reduce_scatter x1, waiting for transfers between devices, body(): lax.psum_scatter((jnp.dot(ret_out, ret_rows, preferred_element_type=jnp.f...  10.2 us
    add x6, other arithmetic, advance(): return (jnp.exp(end_decay)[:, None, None] * carried + fresh_state, carried)  6.24 us
    dynamic_update_slice x6, other arithmetic, body(): lax.scan(advance, empty_state, (block_ends, block_states))  4.36 us
    dot_general x1, matrix products, body(): jnp.einsum('bhst,bthd->bshd', mix_weights, value_blocks, preferred_elemen...  4.33 us
  transfers between devices with their start and end apart: 3, of which 1 were waited for; matrix products, arithmetic and copies ran while one was open for 52% of the time, Pallas kernels for 0%

commit v1 on v0

v1 whole, which is shorter than its diff:
```python
import functools

import jax
import jax.numpy as jnp
from jax import lax
from jax.experimental import pallas as pl
from jax.experimental.pallas import tpu as pltpu
from jax.sharding import PartitionSpec as P

DH = 128
TAPS = 3
SPAN = 128
PACK = 16

epsilon = 1e-06
F32 = jnp.float32
BF16 = jnp.bfloat16


def shifted(value, axis, steps):
    count = lax.axis_size(axis)
    first, last = (max(0, -steps), min(count, count - steps))
    return lax.ppermute(value, axis, [(source, source + steps) for source in range(first, last)])


def swapped(value):
    return lax.ppermute(value, "tp", [(0, 1), (1, 0)])


def turn(vectors, cosines, sines):
    return vectors * cosines + pltpu.roll(vectors, DH // 2, 1) * sines


def contract(left, right, dims):
    return lax.dot_general(left, right, (dims, ((), ())), preferred_element_type=F32)


def call(kernel, grid, in_specs, out_specs, out_shape, flops, scratch=(), limit=28):
    return pl.pallas_call(
        kernel,
        grid_spec=pltpu.PrefetchScalarGridSpec(
            num_scalar_prefetch=1,
            grid=grid,
            in_specs=in_specs,
            out_specs=out_specs,
            scratch_shapes=list(scratch),
        ),
        out_shape=out_shape,
        cost_estimate=pl.CostEstimate(flops=flops, bytes_accessed=flops // 400, transcendentals=0),
        compiler_params=pltpu.CompilerParams(
            dimension_semantics=("arbitrary",) * len(grid), vmem_limit_bytes=limit * 2**20
        ),
    )


def key_value_kernel(chunk, pair, own, other, gain, w_key, w_value, cosines, sines, cum_col,
                     normed, keys, values, starts, total):
    step = pl.program_id(0)
    rows = normed.shape[0]
    half = own.shape[1]

    @pl.when(step == 0)
    def _():
        for begin in range(0, rows, SPAN):
            rng = pl.ds(begin, SPAN)
            mine = own[rng, :].astype(F32)
            theirs = other[rng, :].astype(F32)
            square = jnp.sum(mine * mine + theirs * theirs, axis=-1, keepdims=True)
            scale = lax.rsqrt(square / (2 * half) + epsilon)
            first = pair[0] == 0
            low = jnp.where(first, mine, theirs)
            high = jnp.where(first, theirs, mine)
            normed[rng, :half] = (low * scale * gain[:, :half].astype(F32)).astype(BF16)
            normed[rng, half:] = (high * scale * gain[:, half:].astype(F32)).astype(BF16)

    projected_keys = jnp.dot(normed[...], w_key[...], preferred_element_type=F32)
    projected_values = jnp.dot(normed[...], w_value[...], preferred_element_type=F32)
    values[...] = projected_values.astype(BF16)
    for head in range(w_key.shape[1] // DH):
        lanes = slice(head * DH, (head + 1) * DH)
        turned = turn(projected_keys[:, lanes], cosines[...], sines[...]) * DH ** (-0.5)
        turned = turned.astype(BF16)
        keys[:, lanes] = turned
        state = jnp.zeros((DH, DH), F32)
        decay = jnp.ones((1, 1), F32)
        for index in range(rows // chunk):
            begin = index * chunk
            cum = cum_col[0, begin : begin + chunk, head : head + 1]
            end = cum_col[0, begin + chunk - 1 : begin + chunk, head : head + 1]
            starts[head, index] = state.astype(BF16)
            piece = projected_values[begin : begin + chunk, lanes].astype(BF16).astype(F32)
            weighted = (piece * jnp.exp(end - cum)).astype(BF16)
            state = jnp.exp(end) * state + contract(
                turned[begin : begin + chunk], weighted, ((0,), (0,))
            )
            decay = decay * jnp.exp(end)
        total[head, :DH, :] = state.astype(BF16)
        total[head, DH:, :] = jnp.broadcast_to(decay, (PACK, DH)).astype(BF16)


def gate_kernel(pair, normed, w_in, w_pre, gated):
    entered = jnp.dot(normed[...], w_in[...], preferred_element_type=F32).astype(BF16)
    gate = jnp.dot(normed[...], w_pre[...], preferred_element_type=F32).astype(BF16)
    gated[...] = (gate.astype(F32) * entered.astype(F32)).astype(BF16)


def local_kernel(chunk, pair, normed, w_query, w_post, keys, values, starts, cosines, sines,
                 cum_col, cum_row, queries, local, post):
    rows = normed.shape[0]
    projected = jnp.dot(normed[...], w_query[...], preferred_element_type=F32)
    t_index = lax.broadcasted_iota(jnp.int32, (chunk, chunk), 0)
    s_index = lax.broadcasted_iota(jnp.int32, (chunk, chunk), 1)
    mask = t_index >= s_index
    for head in range(w_query.shape[1] // DH):
        lanes = slice(head * DH, (head + 1) * DH)
        turned = turn(projected[:, lanes], cosines[...], sines[...]).astype(BF16)
        queries[:, lanes] = turned
        for index in range(rows // chunk):
            begin = index * chunk
            rng = slice(begin, begin + chunk)
            query = turned[rng]
            column = cum_col[0, rng, head : head + 1]
            row = cum_row[0, head : head + 1, rng]
            scores = contract(query, keys[rng, lanes], ((1,), (1,)))
            decays = jnp.where(mask, jnp.exp(jnp.minimum(column - row, 0.0)), 0.0)
            mixing = (scores * decays).astype(BF16)
            inside = jnp.dot(mixing, values[rng, lanes], preferred_element_type=F32)
            if index:
                across = jnp.dot(query, starts[head, index], preferred_element_type=F32)
                inside = inside + jnp.exp(column) * across
            local[rng, lanes] = inside
    post[...] = jnp.dot(normed[...], w_post[...], preferred_element_type=F32).astype(BF16)


def finish_kernel(rounds, which, queries, local, reach, gated, before, rim, post, taps, *rest):
    received = rest[:rounds]
    merged = rest[rounds]
    rows = queries.shape[0]
    width = queries.shape[1]
    for head in range(width // DH):
        lanes = slice(head * DH, (head + 1) * DH)
        incoming = received[0][head, :DH, :].astype(F32)
        reached = received[0][head, DH : DH + 1, :].astype(F32)
        for message in received[1:]:
            incoming = incoming + reached * message[head, :DH, :].astype(F32)
            reached = reached * message[head, DH : DH + 1, :].astype(F32)
        across = jnp.dot(queries[:, lanes], incoming.astype(BF16), preferred_element_type=F32)
        retained = local[:, lanes] + reach[:, head : head + 1] * across
        square = jnp.mean(retained * retained, axis=-1, keepdims=True)
        merged[:, lanes] = (retained * lax.rsqrt(square + epsilon)).astype(BF16)
    current = gated[...].astype(F32)
    previous = jnp.where(which[0] == 0, rim[...].astype(F32), before[...].astype(F32))
    extended = jnp.concatenate([previous[PACK - 8 :], current], axis=0)
    convolved = taps[TAPS - 1 : TAPS, :].astype(F32) * current
    for tap in range(TAPS - 1):
        offset = 8 - (TAPS - 1) + tap
        convolved = convolved + taps[tap : tap + 1, :].astype(F32) * extended[offset : offset + rows]
    merged[:, width:] = (post[...].astype(F32) * convolved).astype(BF16)


def first_kernel(which, merged, w_ret, w_conv, partial):
    width = w_ret.shape[0]
    partial[...] = jnp.dot(
        merged[:, :width], w_ret[...], preferred_element_type=F32
    ) + jnp.dot(merged[:, width:], w_conv[...], preferred_element_type=F32)


def second_kernel(which, merged, w_ret, w_conv, partial, mixed):
    width = w_ret.shape[0]
    mixed[...] = (
        partial[...]
        + jnp.dot(merged[:, :width], w_ret[...], preferred_element_type=F32)
        + jnp.dot(merged[:, width:], w_conv[...], preferred_element_type=F32)
    ).astype(BF16)


def body(
    tokens,
    norm_gain,
    w_query,
    w_key,
    w_value,
    log_decay,
    w_conv_in,
    w_conv_pre,
    w_conv_post,
    conv_taps,
    w_out_ret,
    w_out_conv,
):
    other = swapped(tokens)
    rows, half = tokens.shape
    depth = 2 * half
    width = w_query.shape[1]
    conv_width = w_conv_in.shape[1]
    heads = width // DH
    chunk = 2 * SPAN if rows % (2 * SPAN) == 0 else SPAN
    chunks = rows // chunk
    group = 2 if heads % 2 == 0 else 1
    steps = heads // group
    gw = group * DH
    cgw = conv_width // steps
    pair = lax.axis_index("tp").astype(jnp.int32)
    pair_scalar = pair.reshape(1)

    halfway = DH // 2
    positions = lax.axis_index("sp") * rows + jnp.arange(rows, dtype=jnp.int32)
    inverse = 10000.0 ** (-jnp.arange(halfway, dtype=F32) / halfway)
    angles = positions.astype(F32)[:, None] * jnp.concatenate([inverse, inverse])[None, :]
    sign = jnp.where(jnp.arange(DH) < halfway, -1.0, 1.0).astype(F32)
    cosines = jnp.cos(angles)
    sines = jnp.sin(angles) * sign[None, :]

    cumulative = jnp.cumsum(log_decay.reshape(heads, chunks, chunk), axis=-1)
    ends = cumulative[..., -1]
    prefix = jnp.cumsum(ends, axis=-1) - ends
    reach = jnp.exp(cumulative + prefix[..., None]).reshape(heads, rows).T
    cum_row = cumulative.reshape(steps, group, rows)
    cum_col = cum_row.transpose(0, 2, 1)

    full = lambda *shape: pl.BlockSpec(shape, lambda j, s: (0,) * len(shape))
    columns = lambda height, size: pl.BlockSpec((height, size), lambda j, s: (0, j))
    lead = lambda *shape: pl.BlockSpec(shape, lambda j, s: (j,) + (0,) * (len(shape) - 1))
    arr = jax.ShapeDtypeStruct
    unit = 2 * rows * depth * width

    normed, keys, values, starts, total = call(
        functools.partial(key_value_kernel, chunk),
        (steps,),
        [full(rows, half), full(rows, half), full(1, depth), columns(depth, gw), columns(depth, gw),
         full(rows, DH), full(rows, DH), lead(1, rows, group)],
        [full(rows, depth), columns(rows, gw), columns(rows, gw),
         lead(group, chunks, DH, DH), lead(group, DH + PACK, DH)],
        [arr((rows, depth), BF16), arr((rows, width), BF16), arr((rows, width), BF16),
         arr((heads, chunks, DH, DH), BF16), arr((heads, DH + PACK, DH), BF16)],
        2 * unit,
    )(pair_scalar, tokens, other, norm_gain.reshape(1, depth), w_key, w_value, cosines, sines,
      cum_col)

    gated = call(
        gate_kernel,
        (steps,),
        [full(rows, depth), columns(depth, cgw), columns(depth, cgw)],
        columns(rows, cgw),
        arr((rows, conv_width), BF16),
        2 * unit,
    )(pair_scalar, normed, w_conv_in, w_conv_pre)
    rim = shifted(gated[rows - PACK :], "sp", 1)

    received = []
    window = total
    steps_back = 1
    count = lax.axis_size("sp")
    while steps_back < count or not received:
        message = shifted(window, "sp", steps_back)
        received.append(message)
        steps_back *= 2
        if steps_back < count:
            own_decay = window[:, DH : DH + 1, :].astype(F32)
            is_state = (jnp.arange(DH + PACK) < DH)[None, :, None]
            window = (
                jnp.where(is_state, window.astype(F32), 0.0) + own_decay * message.astype(F32)
            ).astype(BF16)

    queries, local, post = call(
        functools.partial(local_kernel, chunk),
        (steps,),
        [full(rows, depth), columns(depth, gw), columns(depth, cgw), columns(rows, gw),
         columns(rows, gw), lead(group, chunks, DH, DH), full(rows, DH), full(rows, DH),
         lead(1, rows, group), lead(1, group, rows)],
        [columns(rows, gw), columns(rows, gw), columns(rows, cgw)],
        [arr((rows, width), BF16), arr((rows, width), F32), arr((rows, conv_width), BF16)],
        3 * unit,
    )(pair_scalar, normed, w_query, w_conv_post, keys, values, starts, cosines, sines, cum_col,
      cum_row)

    part = rows // 2
    blocks_per = part // PACK

    def finish(which):
        piece = lambda size: pl.BlockSpec((part, size), lambda j, s: (s[0], 0))
        return call(
            functools.partial(finish_kernel, len(received)),
            (1,),
            [piece(width), piece(width), piece(heads), piece(conv_width),
             pl.BlockSpec(
                 (PACK, conv_width), lambda j, s: (jnp.maximum(s[0] * blocks_per - 1, 0), 0)
             ),
             full(PACK, conv_width), piece(conv_width), full(TAPS, conv_width)]
            + [full(heads, DH + PACK, DH)] * len(received),
            full(part, width + conv_width),
            arr((part, width + conv_width), BF16),
            unit // 3,
        )(which.reshape(1), queries, local, reach, gated, gated, rim, post, conv_taps, *received)

    to_send = finish(1 - pair)
    arrived = swapped(to_send)
    kept = finish(pair)

    model = w_out_ret.shape[1]
    tile = model // 4
    weight = lambda height: pl.BlockSpec((height, tile), lambda j, s: (s[0], j))
    partial = call(
        first_kernel,
        (model // tile,),
        [full(part, width + conv_width), weight(width), weight(conv_width)],
        columns(part, tile),
        arr((part, model), F32),
        unit,
    )(pair_scalar, kept, w_out_ret, w_out_conv)
    return call(
        second_kernel,
        (model // tile,),
        [full(part, width + conv_width), weight(width), weight(conv_width), columns(part, tile)],
        columns(part, tile),
        arr((part, model), BF16),
        unit,
    )(1 - pair_scalar, arrived, w_out_ret, w_out_conv, partial)


def solution(mesh):
    in_specs = (
        P(("fs", "sp"), "tp"),
        P(),
        P(None, "tp"),
        P(None, "tp"),
        P(None, "tp"),
        P("tp", "sp"),
        P(None, "tp"),
        P(None, "tp"),
        P(None, "tp"),
        P(None, "tp"),
        P(),
        P(),
    )
    out_specs = P(("fs", "sp", "tp"), None)
    return jax.shard_map(body, mesh=mesh, in_specs=in_specs, out_specs=out_specs, check_vma=False)
```

time: 142 us -> 60 us (0.42)
  matrix products: 34.4 us -> 0 us
  Pallas kernels: 0 us -> 29.7 us
  blocking collectives: 29 us -> 0 us
  local copies, waits for them, and re-layouts: 26.8 us -> 6.76 us
  other arithmetic: 23.9 us -> 5.55 us
  between operations: 14.4 us -> 0.31 us
  starting transfers between devices: 1.5 us -> 14.1 us
  waiting for transfers between devices: 10.9 us -> 3.32 us
    dot_general x11 -> x0, matrix products: 34.4 us -> none  [the longest x6 17.8 us: project(): return jnp.dot(normed, weight, preferred_element_type=jnp.float32)]
    pallas_call x0 -> x7, Pallas kernels: none -> 29.7 us  [the longest x1 9.02 us: body(): call(functools.partial(local_kernel, chunk), (steps,), [full(rows, depth)...]
    concatenate x8 -> x0, local copies, waits for them, and re-layouts: 19.3 us -> none  [rotate(): jnp.concatenate([leading * cosines - trailing * sinusoid, leading * sinus...]
    all_gather x1 -> x0, blocking collectives: 15.6 us -> none  [body(): lax.all_gather(local_total[None].astype(jnp.bfloat16), 'sp', axis=0, tile...]
    unnamed x1 -> x0, blocking collectives: 13.5 us -> none
    ppermute x1 -> x3, starting transfers between devices: 1.46 us -> 13.6 us  [shifted(): lax.ppermute(value, axis, [(source, source + steps) for source in range(f...]
    reduce_scatter x1 -> x0, waiting for transfers between devices: 10.2 us -> none  [body(): lax.psum_scatter((jnp.dot(ret_out, ret_rows, preferred_element_type=jnp.f...]
    add x6 -> x0, other arithmetic: 6.24 us -> none  [advance(): return (jnp.exp(end_decay)[:, None, None] * carried + fresh_state, carried)]
  transfers between devices with their start and end apart: 3 -> 5, of which waited for: 1 -> 1; matrix products, arithmetic and copies ran while one was open for 52% -> 13% of each run, Pallas kernels for 0% -> 22%
where the time goes in v1:
time: 60 us; the launch traced here: 59.7 us
  Pallas kernels  29.7 us (50%)
  starting transfers between devices  14.1 us (24%)
  local copies, waits for them, and re-layouts  6.76 us (11%)
  other arithmetic  5.55 us (9%)
  waiting for transfers between devices  3.32 us (6%)
    ppermute x3, starting transfers between devices, shifted(): lax.ppermute(value, axis, [(source, source + steps) for source in range(f...  13.6 us
    pallas_call x1, Pallas kernels, body(): call(functools.partial(local_kernel, chunk), (steps,), [full(rows, depth)...  9.02 us
    pallas_call x1, Pallas kernels, body(): call(functools.partial(key_value_kernel, chunk), (steps,), [full(rows, ha...  7.83 us
    unnamed x20, local copies, waits for them, and re-layouts  4.27 us
    pallas_call x1, Pallas kernels, body(): call(gate_kernel, (steps,), [full(rows, depth), columns(depth, cgw), colu...  3.97 us
    another operation x3, other arithmetic  3.75 us
    pallas_call x1, Pallas kernels, body(): call(second_kernel, (model // tile,), [full(part, width + conv_width), we...  3.68 us
    ppermute x3, waiting for transfers between devices, shifted(): lax.ppermute(value, axis, [(source, source + steps) for source in range(f...  3.32 us
  transfers between devices with their start and end apart: 5, of which 1 were waited for; matrix products, arithmetic and copies ran while one was open for 13% of the time, Pallas kernels for 22%

profile of v1, /device:TPU:0, one launch (start us, length us, event | category | flops | bytes accessed | tf_op | source)
XLA Modules:
  0.0 59.7 jit_solution(11819389751260217925)
XLA Ops:
  0.0 0.5 collective-permute-start
  0.5 0.9 %reshape.53 = f32[4,3,2,128]{3,2,1,0:T(2,128)S(1)} reshape(f32[4,768]{1,0:T(4,128)} %param.17) | data formatting | bytes 24576 | tf_op jit(solution)/shard_map/reshape
  1.4 3.6 %reduce-window.6 = f32[4,3,2,128]{3,2,1,0:T(2,128)S(1)} reduce-window(f32[4,3,2,128]{3,2,1,0:T(2,128)S(1)} %reshape.53, f32[]{:T(128)} %constant.34.clone.1), window={size=1x1x1x128 pad=0_0x0_0x0_0x127_0}, to_apply=%region_0.1 | reduce-window | flops 390144 | bytes 24580 | tf_op jit(solution)/shard_map/reduce-window
  5.0 0.1 slice.20
  5.1 0.1 copy.20
  5.2 0.1 copy.21
  5.3 0.1 broadcast_add_fusion
  5.5 0.2 copy.24
  5.7 0.7 %reshape.52.gain = bf16[1,2048]{1,0:T(2,128)(2,1)S(1)} reshape(bf16[2048]{0:T(1024)(128)(2,1)} %param.13) | data formatting | bytes 8192 | tf_op jit(solution)/shard_map/reshape | solution.py:237
  6.4 0.3 copy.22.cum_col
  6.7 0.1 reduce-window_subtract_fusion
  6.7 0.1 copy.28
  6.8 0.1 fusion.1
  7.0 0.1 compare_select_fusion
  7.0 1.4 %fusion = (f32[768,128]{1,0:T(8,128)S(1)}, f32[768,128]{1,0:T(8,128)S(1)}) fusion(f32[128]{0:T(128)S(1)} %get-tuple-element.23, f32[128]{0:T(128)S(1)} %get-tuple-element.24, f32[768]{0:T(1024)S(1)} %add_convert_fusion.1), kind=kLoop, calls=%fused_computation.3 | loop fusion | flops 196608 | bytes 790528 | tf_op jit(solution)/shard_map/mul | solution.py:212
  8.5 0.0 collective-permute-done.other
  8.5 0.0 copy-done.3
  8.5 0.0 copy-start.4
  8.5 1.6 %copy-done.4 = bf16[2048,512]{1,0:T(8,128)(2,1)S(1)} copy-done((bf16[2048,512]{1,0:T(8,128)(2,1)S(1)}, bf16[2048,512]{1,0:T(8,128)(2,1)}, u32[]{:S(2)}) %copy-start.4) | copy-done | bytes 2097176
  10.1 1.4 %copy-done.9 = bf16[768,1024]{1,0:T(8,128)(2,1)S(1)} copy-done((bf16[768,1024]{1,0:T(8,128)(2,1)S(1)}, bf16[768,1024]{1,0:T(8,128)(2,1)}, u32[]{:S(2)}) %copy-start.9) | copy-done | bytes 1572888
  11.5 7.8 %shard_map.118 = (bf16[768,2048]{1,0:T(8,128)(2,1)S(1)}, bf16[768,512]{1,0:T(8,128)(2,1)S(1)}, bf16[768,512]{1,0:T(8,128)(2,1)S(1)}, bf16[4,3,128,128]{3,2,1,0:T(8,128)(2,1)S(1)}, bf16[4,144,128]{2,1,0:T(8,128)(2,1)S(1)}) custom-call(s32[1]{0:T(128)} %bitcast.pair.which, bf16[768,1024]{1,0:T(8,128)(2,1)S(1)} %copy-done.9, ...), custom_call_target="tpu_custom_call" | custom-call | flops 3221225472 | bytes 8053063 | tf_op jit(solution)/shard_map/pallas_call | solution.py:227
  19.4 0.0 copy-done.5
  19.4 0.0 copy-done.6
  19.4 0.0 copy-start.7
  19.4 0.0 copy-start.8
  19.4 4.0 %shard_map.120.gated.before = bf16[768,512]{1,0:T(8,128)(2,1)S(1)} custom-call(s32[1]{0:T(128)} %bitcast.pair.which, bf16[768,2048]{1,0:T(8,128)(2,1)S(1)} %get-tuple-element.13.normed, bf16[2048,512]{1,0:T(8,128)(2,1)S(1)} %copy-done.5, bf16[2048,512]{1,0:T(8,128)(2,1)S(1)} %copy-done.6), custom_call_target="tpu_custom_call" | custom-call | flops 3221225472 | bytes 8053063 | tf_op jit(solution)/shard_map/pallas_call | solution.py:240
  23.4 4.5 %collective-permute-start.1 = (bf16[16,512]{1,0:T(8,128)(2,1)S(1)}, bf16[16,512]{1,0:T(8,128)(2,1)S(1)}, u32[]{:S(2)}, u32[]{:S(2)}) collective-permute-start(bf16[16,512]{1,0:T(8,128)(2,1)S(1)} %slice.23), channel_id=1, source_target_pairs={{0,8},{8,16},{16,24},{1,9},{9,17},{17,25},{2,10},{10,18},{18,26},{... | collective-permute-start | bytes 49160 | tf_op jit(solution)/shard_map/ppermute | solution.py:23
  27.9 3.5 %collective-permute-start.2 = (bf16[4,144,128]{2,1,0:T(8,128)(2,1)S(1)}, bf16[4,144,128]{2,1,0:T(8,128)(2,1)S(1)}, u32[]{:S(2)}, u32[]{:S(2)}) collective-permute-start(bf16[4,144,128]{2,1,0:T(8,128)(2,1)S(1)} %get-tuple-element.20), channel_id=1, source_target_pairs={{0,8},{8,16},{16,24},{1,9},{9,17},{17,25},{2,10},{10,18},{18,26},{... | collective-permute-start | bytes 442376 | tf_op jit(solution)/shard_map/ppermute | solution.py:23
  31.4 3.3 %collective-permute-done.2.rest_0_ = bf16[4,144,128]{2,1,0:T(8,128)(2,1)S(1)} collective-permute-done((bf16[4,144,128]{2,1,0:T(8,128)(2,1)S(1)}, bf16[4,144,128]{2,1,0:T(8,128)(2,1)S(1)}, u32[]{:S(2)}, u32[]{:S(2)}) %collective-permute-start.2) | collective-permute-done | bytes 147488 | tf_op jit(solution)/shard_map/ppermute | solution.py:23
  34.7 0.1 add_convert_fusion
  34.8 5.6 %collective-permute-start.3 = (bf16[4,144,128]{2,1,0:T(8,128)(2,1)S(1)}, bf16[4,144,128]{2,1,0:T(8,128)(2,1)S(1)}, u32[]{:S(2)}, u32[]{:S(2)}) collective-permute-start(bf16[4,144,128]{2,1,0:T(8,128)(2,1)S(1)} %add_convert_fusion), channel_id=1, source_target_pairs={{0,16},{8,24},{1,17},{9,25},{2,18},{10,26},{3,19},{11,27},{4,20},{... | collective-permute-start | bytes 442376 | tf_op jit(solution)/shard_map/ppermute | solution.py:23
  40.4 0.0 copy-done.7
  40.4 0.0 copy-done.8
  40.4 0.0 copy-start.2
  40.5 9.0 %shard_map.119 = (bf16[768,512]{1,0:T(8,128)(2,1)S(1)}, f32[768,512]{1,0:T(8,128)S(1)}, bf16[768,512]{1,0:T(8,128)(2,1)S(1)}) custom-call(s32[1]{0:T(128)} %bitcast.pair.which, bf16[768,2048]{1,0:T(8,128)(2,1)S(1)} %get-tuple-element.13.normed, bf16[2048,512]{1,0:T(8,128)(2,1)S(1)} %copy-done.7, bf16[2048,512]{1,0:T(8,128)(2,1)S(1)} %copy-done.8, ...), custom_call_target="tpu_custom_call" | custom-call | flops 4831838208 | bytes 12079595 | tf_op jit(solution)/shard_map/pallas_call | solution.py:265
  49.5 0.0 collective-permute-done.1.rim
  49.5 0.0 collective-permute-done.3.rest_1_
  49.5 0.0 copy-done.2
  49.5 0.0 copy-start.1
  49.5 1.2 %shard_map.121 = bf16[384,1024]{1,0:T(8,128)(2,1)S(1)} custom-call(s32[1]{0:T(128)} %bitcast.1.which, bf16[768,512]{1,0:T(8,128)(2,1)S(1)} %get-tuple-element.17.queries, f32[768,512]{1,0:T(8,128)S(1)} %get-tuple-element.18.local, f32[768,4]{1,0:T(8,128)S(1)} %bitcast.17, bf16[768,512]{1,0:T(8,128)(2,1)S(1)} %shard_map.120.gated.before, ...), custom_call_target="tpu_custom_call" | custom-call | flops 536870912 | bytes 1342177 | tf_op jit(solution)/shard_map/pallas_call | solution.py:282
  50.7 0.1 collective-permute-start.4
  50.8 0.0 copy-start
  50.8 1.2 %shard_map.122.merged = bf16[384,1024]{1,0:T(8,128)(2,1)S(1)} custom-call(s32[1]{0:T(128)} %bitcast.pair.which, bf16[768,512]{1,0:T(8,128)(2,1)S(1)} %get-tuple-element.17.queries, f32[768,512]{1,0:T(8,128)S(1)} %get-tuple-element.18.local, f32[768,4]{1,0:T(8,128)S(1)} %bitcast.18, bf16[768,512]{1,0:T(8,128)(2,1)S(1)} %shard_map.120.gated.before, ...), custom_call_target="tpu_custom_call" | custom-call | flops 536870912 | bytes 1342177 | tf_op jit(solution)/shard_map/pallas_call | solution.py:282
  52.0 0.0 copy-done.1
  52.0 1.2 %copy-done = bf16[1024,2048]{1,0:T(8,128)(2,1)S(1)} copy-done((bf16[1024,2048]{1,0:T(8,128)(2,1)S(1)}, bf16[1024,2048]{1,0:T(8,128)(2,1)}, u32[]{:S(2)}) %copy-start) | copy-done | bytes 4194328
  53.2 2.8 %shard_map.123.partial = f32[384,2048]{1,0:T(8,128)S(1)} custom-call(s32[1]{0:T(128)} %bitcast.pair.which, bf16[384,1024]{1,0:T(8,128)(2,1)S(1)} %shard_map.122.merged, bf16[1024,2048]{1,0:T(8,128)(2,1)S(1)} %copy-done, bf16[1024,2048]{1,0:T(8,128)(2,1)S(1)} %copy-done.1), custom_call_target="tpu_custom_call" | custom-call | flops 1610612736 | bytes 4026531 | tf_op jit(solution)/shard_map/pallas_call | solution.py:303
  56.1 0.0 collective-permute-done.4.merged
  56.1 3.7 %shard_map.124 = bf16[384,2048]{1,0:T(8,128)(2,1)} custom-call(s32[1]{0:T(128)S(6)} %sub.10.which, bf16[384,1024]{1,0:T(8,128)(2,1)S(1)} %collective-permute-done.4.merged, bf16[1024,2048]{1,0:T(8,128)(2,1)S(1)} %copy-done, bf16[1024,2048]{1,0:T(8,128)(2,1)S(1)} %copy-done.1, f32[384,2048]{1,0:T(8,128)S(1)} %shard_map.123.partial), custom_call_target="tpu_custom_call" | custom-call | flops 1610612736 | bytes 4026531 | tf_op jit(solution)/shard_map/pallas_call | solution.py:311
  (13 shorter events, 0.1 us)
Async XLA Ops:
  0.0 8.5 %copy-start.3 = (bf16[2048,512]{1,0:T(8,128)(2,1)S(1)}, bf16[2048,512]{1,0:T(8,128)(2,1)}, u32[]{:S(2)}) copy-start(bf16[2048,512]{1,0:T(8,128)(2,1)} %w_key.1) | copy-start | bytes 6291460
  0.0 8.5 %collective-permute-start = (bf16[768,1024]{1,0:T(8,128)(2,1)}, bf16[768,1024]{1,0:T(8,128)(2,1)}, u32[]{:S(2)}, u32[]{:S(2)}) collective-permute-start(bf16[768,1024]{1,0:T(8,128)(2,1)} %own.1), channel_id=1, source_target_pairs={{0,1},{1,0},{2,3},{3,2},{4,5},{5,4},{6,7},{7,6},{8,9},{9,8},{10,11... | collective-permute-start | bytes 4718600 | tf_op jit(solution)/shard_map/ppermute | solution.py:27
  8.5 1.6 %copy-start.4 = (bf16[2048,512]{1,0:T(8,128)(2,1)S(1)}, bf16[2048,512]{1,0:T(8,128)(2,1)}, u32[]{:S(2)}) copy-start(bf16[2048,512]{1,0:T(8,128)(2,1)} %w_value.1) | copy-start | bytes 6291460
  10.1 1.4 %copy-start.9 = (bf16[768,1024]{1,0:T(8,128)(2,1)S(1)}, bf16[768,1024]{1,0:T(8,128)(2,1)}, u32[]{:S(2)}) copy-start(bf16[768,1024]{1,0:T(8,128)(2,1)} %own.1) | copy-start | bytes 4718596
  11.5 7.8 %copy-start.5 = (bf16[2048,512]{1,0:T(8,128)(2,1)S(1)}, bf16[2048,512]{1,0:T(8,128)(2,1)}, u32[]{:S(2)}) copy-start(bf16[2048,512]{1,0:T(8,128)(2,1)} %w_in.1) | copy-start | bytes 6291460
  11.5 7.9 %copy-start.6 = (bf16[2048,512]{1,0:T(8,128)(2,1)S(1)}, bf16[2048,512]{1,0:T(8,128)(2,1)}, u32[]{:S(2)}) copy-start(bf16[2048,512]{1,0:T(8,128)(2,1)} %w_pre.1) | copy-start | bytes 6291460
  19.4 21.1 %copy-start.7 = (bf16[2048,512]{1,0:T(8,128)(2,1)S(1)}, bf16[2048,512]{1,0:T(8,128)(2,1)}, u32[]{:S(2)}) copy-start(bf16[2048,512]{1,0:T(8,128)(2,1)} %w_query.1) | copy-start | bytes 6291460
  19.4 21.0 %copy-start.8 = (bf16[2048,512]{1,0:T(8,128)(2,1)S(1)}, bf16[2048,512]{1,0:T(8,128)(2,1)}, u32[]{:S(2)}) copy-start(bf16[2048,512]{1,0:T(8,128)(2,1)} %w_post.1) | copy-start | bytes 6291460
  23.4 26.1 %collective-permute-start.1 = (bf16[16,512]{1,0:T(8,128)(2,1)S(1)}, bf16[16,512]{1,0:T(8,128)(2,1)S(1)}, u32[]{:S(2)}, u32[]{:S(2)}) collective-permute-start(bf16[16,512]{1,0:T(8,128)(2,1)S(1)} %slice.23), channel_id=1, source_target_pairs={{0,8},{8,16},{16,24},{1,9},{9,17},{17,25},{2,10},{10,18},{18,26},{... | collective-permute-start | bytes 49160 | tf_op jit(solution)/shard_map/ppermute | solution.py:23
  27.9 6.8 %collective-permute-start.2 = (bf16[4,144,128]{2,1,0:T(8,128)(2,1)S(1)}, bf16[4,144,128]{2,1,0:T(8,128)(2,1)S(1)}, u32[]{:S(2)}, u32[]{:S(2)}) collective-permute-start(bf16[4,144,128]{2,1,0:T(8,128)(2,1)S(1)} %get-tuple-element.20), channel_id=1, source_target_pairs={{0,8},{8,16},{16,24},{1,9},{9,17},{17,25},{2,10},{10,18},{18,26},{... | collective-permute-start | bytes 442376 | tf_op jit(solution)/shard_map/ppermute | solution.py:23
  34.8 14.7 %collective-permute-start.3 = (bf16[4,144,128]{2,1,0:T(8,128)(2,1)S(1)}, bf16[4,144,128]{2,1,0:T(8,128)(2,1)S(1)}, u32[]{:S(2)}, u32[]{:S(2)}) collective-permute-start(bf16[4,144,128]{2,1,0:T(8,128)(2,1)S(1)} %add_convert_fusion), channel_id=1, source_target_pairs={{0,16},{8,24},{1,17},{9,25},{2,18},{10,26},{3,19},{11,27},{4,20},{... | collective-permute-start | bytes 442376 | tf_op jit(solution)/shard_map/ppermute | solution.py:23
  40.4 9.1 %copy-start.2 = (bf16[3,512]{1,0:T(4,128)(2,1)S(1)}, bf16[3,512]{1,0:T(4,128)(2,1)}, u32[]{:S(2)}) copy-start(bf16[3,512]{1,0:T(4,128)(2,1)} %taps.3) | copy-start | bytes 9220
  49.5 2.4 %copy-start.1 = (bf16[1024,2048]{1,0:T(8,128)(2,1)S(1)}, bf16[1024,2048]{1,0:T(8,128)(2,1)}, u32[]{:S(2)}) copy-start(bf16[1024,2048]{1,0:T(8,128)(2,1)} %w_conv.3) | copy-start | bytes 12582916
  50.7 5.4 %collective-permute-start.4 = (bf16[384,1024]{1,0:T(8,128)(2,1)S(1)}, bf16[384,1024]{1,0:T(8,128)(2,1)S(1)}, u32[]{:S(2)}, u32[]{:S(2)}) collective-permute-start(bf16[384,1024]{1,0:T(8,128)(2,1)S(1)} %shard_map.121), channel_id=1, source_target_pairs={{0,1},{1,0},{2,3},{3,2},{4,5},{5,4},{6,7},{7,6},{8,9},{9,8},{10,11... | collective-permute-start | bytes 2359304 | tf_op jit(solution)/shard_map/ppermute | solution.py:27
  50.8 2.4 %copy-start = (bf16[1024,2048]{1,0:T(8,128)(2,1)S(1)}, bf16[1024,2048]{1,0:T(8,128)(2,1)}, u32[]{:S(2)}) copy-start(bf16[1024,2048]{1,0:T(8,128)(2,1)} %w_ret.3) | copy-start | bytes 12582916

commit v2 on v1

v2 whole, which is shorter than its diff:
```python
import functools

import jax
import jax.numpy as jnp
from jax import lax
from jax.experimental import pallas as pl
from jax.experimental.pallas import tpu as pltpu
from jax.sharding import PartitionSpec as P

DH = 128
TAPS = 3
SPAN = 128
PACK = 16

epsilon = 1e-06
F32 = jnp.float32
BF16 = jnp.bfloat16


def shifted(value, axis, steps):
    count = lax.axis_size(axis)
    first, last = (max(0, -steps), min(count, count - steps))
    return lax.ppermute(value, axis, [(source, source + steps) for source in range(first, last)])


def swapped(value):
    return lax.ppermute(value, "tp", [(0, 1), (1, 0)])


def turn(vectors, cosines, sines):
    return vectors * cosines + pltpu.roll(vectors, DH // 2, 1) * sines


def contract(left, right, dims):
    return lax.dot_general(left, right, (dims, ((), ())), preferred_element_type=F32)


def call(kernel, grid, in_specs, out_specs, out_shape, flops, scratch=(), limit=28):
    return pl.pallas_call(
        kernel,
        grid_spec=pltpu.PrefetchScalarGridSpec(
            num_scalar_prefetch=1,
            grid=grid,
            in_specs=in_specs,
            out_specs=out_specs,
            scratch_shapes=list(scratch),
        ),
        out_shape=out_shape,
        cost_estimate=pl.CostEstimate(flops=flops, bytes_accessed=flops // 400, transcendentals=0),
        compiler_params=pltpu.CompilerParams(
            dimension_semantics=("arbitrary",) * len(grid), vmem_limit_bytes=limit * 2**20
        ),
    )


def project(pair, normed, weight):
    half = normed.shape[1] // 2
    mine = pl.multiple_of(pair[0] * half, half)
    theirs = pl.multiple_of((1 - pair[0]) * half, half)
    return jnp.dot(
        normed[:, :half], weight[pl.ds(mine, half), :], preferred_element_type=F32
    ) + jnp.dot(normed[:, half:], weight[pl.ds(theirs, half), :], preferred_element_type=F32)


def decay_kernel(chunk, group, pair, log_decay, cum_row, cum_col, reach):
    heads, rows = log_decay.shape
    first = lax.broadcasted_iota(jnp.int32, (chunk, chunk), 0)
    second = lax.broadcasted_iota(jnp.int32, (chunk, chunk), 1)
    upper = (first <= second).astype(F32)
    lower = (first >= second).astype(F32)
    prefix = jnp.zeros((1, heads), F32)
    for begin in range(0, rows, chunk):
        rng = slice(begin, begin + chunk)
        piece = log_decay[:, rng]
        row = jnp.dot(piece, upper, precision=lax.Precision.HIGHEST, preferred_element_type=F32)
        column = lax.dot_general(
            lower, piece, (((1,), (1,)), ((), ())),
            precision=lax.Precision.HIGHEST, preferred_element_type=F32,
        )
        for step in range(heads // group):
            cum_row[step, :, rng] = row[step * group : (step + 1) * group]
            cum_col[step, rng, :] = column[:, step * group : (step + 1) * group]
        reach[rng, :] = jnp.exp(column + prefix)
        prefix = prefix + column[chunk - 1 : chunk, :]


def key_value_kernel(chunk, pair, own, other, gain, w_key, w_value, cosines, sines, cum_col,
                     normed, keys, values, starts, total):
    step = pl.program_id(0)
    rows = normed.shape[0]
    half = own.shape[1]

    @pl.when(step == 0)
    def _():
        low_gain = gain[0:1, :].astype(F32)
        high_gain = gain[1:2, :].astype(F32)
        my_gain = jnp.where(pair[0] == 0, low_gain, high_gain)
        their_gain = jnp.where(pair[0] == 0, high_gain, low_gain)
        for begin in range(0, rows, SPAN):
            rng = pl.ds(begin, SPAN)
            mine = own[rng, :].astype(F32)
            theirs = other[rng, :].astype(F32)
            square = jnp.sum(mine * mine + theirs * theirs, axis=-1, keepdims=True)
            scale = lax.rsqrt(square / (2 * half) + epsilon)
            normed[rng, :half] = (mine * scale * my_gain).astype(BF16)
            normed[rng, half:] = (theirs * scale * their_gain).astype(BF16)

    projected_keys = project(pair, normed, w_key)
    projected_values = project(pair, normed, w_value)
    values[...] = projected_values.astype(BF16)
    for head in range(w_key.shape[1] // DH):
        lanes = slice(head * DH, (head + 1) * DH)
        turned = turn(projected_keys[:, lanes], cosines[...], sines[...]) * DH ** (-0.5)
        turned = turned.astype(BF16)
        keys[:, lanes] = turned
        state = jnp.zeros((DH, DH), F32)
        decay = jnp.ones((1, 1), F32)
        for index in range(rows // chunk):
            begin = index * chunk
            cum = cum_col[0, begin : begin + chunk, head : head + 1]
            end = cum_col[0, begin + chunk - 1 : begin + chunk, head : head + 1]
            starts[head, index] = state.astype(BF16)
            piece = projected_values[begin : begin + chunk, lanes].astype(BF16).astype(F32)
            weighted = (piece * jnp.exp(end - cum)).astype(BF16)
            state = jnp.exp(end) * state + contract(
                turned[begin : begin + chunk], weighted, ((0,), (0,))
            )
            decay = decay * jnp.exp(end)
        total[:DH, lanes] = state.astype(BF16)
        total[DH:, lanes] = jnp.broadcast_to(decay, (PACK, DH)).astype(BF16)


def gate_kernel(pair, normed, w_in, w_pre, total, gated, message):
    entered = project(pair, normed, w_in).astype(BF16)
    gate = project(pair, normed, w_pre).astype(BF16)
    product = (gate.astype(F32) * entered.astype(F32)).astype(BF16)
    gated[...] = product
    message[: DH + PACK, :] = total[...]
    message[DH + PACK :, :] = product[product.shape[0] - PACK :, :]


def query_kernel(pair, normed, w_query, w_post, cosines, sines, queries, post):
    projected = project(pair, normed, w_query)
    for head in range(w_query.shape[1] // DH):
        lanes = slice(head * DH, (head + 1) * DH)
        queries[:, lanes] = turn(projected[:, lanes], cosines[...], sines[...]).astype(BF16)
    post[...] = project(pair, normed, w_post).astype(BF16)


def local_kernel(chunk, pair, queries, keys, values, starts, cum_col, cum_row, local):
    rows = queries.shape[0]
    t_index = lax.broadcasted_iota(jnp.int32, (chunk, chunk), 0)
    s_index = lax.broadcasted_iota(jnp.int32, (chunk, chunk), 1)
    mask = t_index >= s_index
    for head in range(queries.shape[1] // DH):
        lanes = slice(head * DH, (head + 1) * DH)
        for index in range(rows // chunk):
            begin = index * chunk
            rng = slice(begin, begin + chunk)
            query = queries[rng, lanes]
            column = cum_col[0, rng, head : head + 1]
            row = cum_row[0, head : head + 1, rng]
            scores = contract(query, keys[rng, lanes], ((1,), (1,)))
            decays = jnp.where(mask, jnp.exp(jnp.minimum(column - row, 0.0)), 0.0)
            mixing = (scores * decays).astype(BF16)
            inside = jnp.dot(mixing, values[rng, lanes], preferred_element_type=F32)
            if index:
                across = jnp.dot(query, starts[head, index], preferred_element_type=F32)
                inside = inside + jnp.exp(column) * across
            local[rng, lanes] = inside


def finish_kernel(rounds, which, queries, local, reach, gated, before, post, taps, *rest):
    received = rest[:rounds]
    merged = rest[rounds]
    rows = queries.shape[0]
    width = queries.shape[1]
    for head in range(width // DH):
        lanes = slice(head * DH, (head + 1) * DH)
        incoming = received[0][:DH, lanes].astype(F32)
        reached = received[0][DH : DH + 1, lanes].astype(F32)
        for message in received[1:]:
            incoming = incoming + reached * message[:DH, lanes].astype(F32)
            reached = reached * message[DH : DH + 1, lanes].astype(F32)
        across = jnp.dot(queries[:, lanes], incoming.astype(BF16), preferred_element_type=F32)
        retained = local[:, lanes] + reach[:, head : head + 1] * across
        square = jnp.mean(retained * retained, axis=-1, keepdims=True)
        merged[:, lanes] = (retained * lax.rsqrt(square + epsilon)).astype(BF16)
    current = gated[...].astype(F32)
    previous = jnp.where(which[0] == 0, received[0][DH + PACK :, :].astype(F32), before[...].astype(F32))
    extended = jnp.concatenate([previous[PACK - 8 :], current], axis=0)
    convolved = taps[TAPS - 1 : TAPS, :].astype(F32) * current
    for tap in range(TAPS - 1):
        offset = 8 - (TAPS - 1) + tap
        convolved = convolved + taps[tap : tap + 1, :].astype(F32) * extended[offset : offset + rows]
    merged[:, width:] = (post[...].astype(F32) * convolved).astype(BF16)


def output_kernel(pair, kept, arrived, w_ret, w_conv, mixed):
    width = w_ret.shape[0] // 2
    mine = pl.multiple_of(pair[0] * width, width)
    theirs = pl.multiple_of((1 - pair[0]) * width, width)
    mixed[...] = (
        jnp.dot(kept[:, :width], w_ret[pl.ds(mine, width), :], preferred_element_type=F32)
        + jnp.dot(kept[:, width:], w_conv[pl.ds(mine, width), :], preferred_element_type=F32)
        + jnp.dot(arrived[:, :width], w_ret[pl.ds(theirs, width), :], preferred_element_type=F32)
        + jnp.dot(arrived[:, width:], w_conv[pl.ds(theirs, width), :], preferred_element_type=F32)
    ).astype(BF16)


def body(
    tokens,
    norm_gain,
    w_query,
    w_key,
    w_value,
    log_decay,
    w_conv_in,
    w_conv_pre,
    w_conv_post,
    conv_taps,
    w_out_ret,
    w_out_conv,
):
    other = swapped(tokens)
    rows, half = tokens.shape
    depth = 2 * half
    width = w_query.shape[1]
    conv_width = w_conv_in.shape[1]
    heads = width // DH
    chunk = 2 * SPAN if rows % (2 * SPAN) == 0 else SPAN
    chunks = rows // chunk
    group = 2 if heads % 2 == 0 else 1
    steps = heads // group
    gw = group * DH
    cgw = conv_width // steps
    pair = lax.axis_index("tp").astype(jnp.int32)
    pair_scalar = pair.reshape(1)

    halfway = DH // 2
    positions = lax.axis_index("sp") * rows + jnp.arange(rows, dtype=jnp.int32)
    inverse = 10000.0 ** (-jnp.arange(halfway, dtype=F32) / halfway)
    angles = positions.astype(F32)[:, None] * jnp.concatenate([inverse, inverse])[None, :]
    sign = jnp.where(jnp.arange(DH) < halfway, -1.0, 1.0).astype(F32)
    cosines = jnp.cos(angles)
    sines = jnp.sin(angles) * sign[None, :]

    full = lambda *shape: pl.BlockSpec(shape, lambda j, s: (0,) * len(shape))
    columns = lambda height, size: pl.BlockSpec((height, size), lambda j, s: (0, j))
    lead = lambda *shape: pl.BlockSpec(shape, lambda j, s: (j,) + (0,) * (len(shape) - 1))
    arr = jax.ShapeDtypeStruct
    unit = 2 * rows * depth * width

    cum_row, cum_col, reach = call(
        functools.partial(decay_kernel, chunk, group),
        (1,),
        [full(heads, rows)],
        [full(steps, group, rows), full(steps, rows, group), full(rows, heads)],
        [arr((steps, group, rows), F32), arr((steps, rows, group), F32), arr((rows, heads), F32)],
        unit // 8,
    )(pair_scalar, log_decay)

    normed, keys, values, starts, total = call(
        functools.partial(key_value_kernel, chunk),
        (steps,),
        [full(rows, half), full(rows, half), full(2, half), columns(depth, gw), columns(depth, gw),
         full(rows, DH), full(rows, DH), lead(1, rows, group)],
        [full(rows, depth), columns(rows, gw), columns(rows, gw),
         lead(group, chunks, DH, DH), columns(DH + PACK, gw)],
        [arr((rows, depth), BF16), arr((rows, width), BF16), arr((rows, width), BF16),
         arr((heads, chunks, DH, DH), BF16), arr((DH + PACK, width), BF16)],
        2 * unit,
    )(pair_scalar, tokens, other, norm_gain.reshape(2, half), w_key, w_value, cosines, sines,
      cum_col)

    gated, window = call(
        gate_kernel,
        (steps,),
        [full(rows, depth), columns(depth, cgw), columns(depth, cgw), columns(DH + PACK, gw)],
        [columns(rows, cgw), columns(DH + 2 * PACK, gw)],
        [arr((rows, conv_width), BF16), arr((DH + 2 * PACK, width), BF16)],
        2 * unit,
    )(pair_scalar, normed, w_conv_in, w_conv_pre, total)

    received = []
    steps_back = 1
    count = lax.axis_size("sp")
    while steps_back < count or not received:
        message = shifted(window, "sp", steps_back)
        received.append(message)
        steps_back *= 2
        if steps_back < count:
            own_decay = window[DH : DH + 1, :].astype(F32)
            is_state = (jnp.arange(DH + PACK) < DH)[:, None]
            window = (
                jnp.where(is_state, window[: DH + PACK].astype(F32), 0.0)
                + own_decay * message[: DH + PACK].astype(F32)
            ).astype(BF16)

    queries, post = call(
        query_kernel,
        (steps,),
        [full(rows, depth), columns(depth, gw), columns(depth, cgw), full(rows, DH),
         full(rows, DH)],
        [columns(rows, gw), columns(rows, cgw)],
        [arr((rows, width), BF16), arr((rows, conv_width), BF16)],
        2 * unit,
    )(pair_scalar, normed, w_query, w_conv_post, cosines, sines)
    local = call(
        functools.partial(local_kernel, chunk),
        (steps,),
        [columns(rows, gw), columns(rows, gw), columns(rows, gw), lead(group, chunks, DH, DH),
         lead(1, rows, group), lead(1, group, rows)],
        columns(rows, gw),
        arr((rows, width), F32),
        2 * unit,
    )(pair_scalar, queries, keys, values, starts, cum_col, cum_row)

    part = rows // 2
    blocks_per = part // PACK

    def finish(which):
        piece = lambda size: pl.BlockSpec((part, size), lambda j, s: (s[0], 0))
        return call(
            functools.partial(finish_kernel, len(received)),
            (1,),
            [piece(width), piece(width), piece(heads), piece(conv_width),
             pl.BlockSpec(
                 (PACK, conv_width), lambda j, s: (jnp.maximum(s[0] * blocks_per - 1, 0), 0)
             ),
             piece(conv_width), full(TAPS, conv_width)]
            + [full(*message.shape) for message in received],
            full(part, width + conv_width),
            arr((part, width + conv_width), BF16),
            unit // 3,
        )(which.reshape(1), queries, local, reach, gated, gated, post, conv_taps, *received)

    to_send = finish(1 - pair)
    arrived = swapped(to_send)
    kept = finish(pair)

    model = w_out_ret.shape[1]
    tile = model // 4
    merged_width = width + conv_width
    return call(
        output_kernel,
        (model // tile,),
        [full(part, merged_width), full(part, merged_width),
         columns(w_out_ret.shape[0], tile), columns(w_out_conv.shape[0], tile)],
        columns(part, tile),
        arr((part, model), BF16),
        2 * unit,
    )(pair_scalar, kept, arrived, w_out_ret, w_out_conv)


def solution(mesh):
    in_specs = (
        P(("fs", "sp"), "tp"),
        P(),
        P(None, "tp"),
        P(None, "tp"),
        P(None, "tp"),
        P("tp", "sp"),
        P(None, "tp"),
        P(None, "tp"),
        P(None, "tp"),
        P(None, "tp"),
        P(),
        P(),
    )
    out_specs = P(("fs", "sp", "tp"), None)
    return jax.shard_map(body, mesh=mesh, in_specs=in_specs, out_specs=out_specs, check_vma=False)
```

time: 60 us -> 48.6 us (0.81)
  the two profiles are of different devices: /device:TPU:0 before, /device:TPU:29 now
where the time goes in v2:
time: 48.6 us; the launch traced here: 48.2 us
  Pallas kernels  25.7 us (53%)
  waiting for transfers between devices  10.6 us (22%)
  local copies, waits for them, and re-layouts  6.05 us (12%)
  starting transfers between devices  4 us (8%)
  other arithmetic  1.66 us (3%)
    ppermute x2, waiting for transfers between devices, shifted(): lax.ppermute(value, axis, [(source, source + steps) for source in range(f...  9.9 us
    pallas_call x1, Pallas kernels, body(): call(functools.partial(key_value_kernel, chunk), (steps,), [full(rows, ha...  6.21 us
    pallas_call x1, Pallas kernels, body(): call(output_kernel, (model // tile,), [full(part, merged_width), full(par...  5.44 us
    unnamed x22, local copies, waits for them, and re-layouts  5.35 us
    pallas_call x1, Pallas kernels, body(): call(query_kernel, (steps,), [full(rows, depth), columns(depth, gw), colu...  4.21 us
    pallas_call x1, Pallas kernels, body(): call(gate_kernel, (steps,), [full(rows, depth), columns(depth, cgw), colu...  4.07 us
    ppermute x2, starting transfers between devices, shifted(): lax.ppermute(value, axis, [(source, source + steps) for source in range(f...  2.76 us
    pallas_call x2, Pallas kernels, finish(): call(functools.partial(finish_kernel, len(received)), (1,), [piece(width)...  2.35 us
  transfers between devices with their start and end apart: 4, of which 3 were waited for; matrix products, arithmetic and copies ran while one was open for 5% of the time, Pallas kernels for 18%

profile of v2, /device:TPU:29, one launch (start us, length us, event | category | flops | bytes accessed | tf_op | source)
XLA Modules:
  0.0 48.2 jit_solution(10507864314515108285)
XLA Ops:
  0.0 0.7 %collective-permute-start = (bf16[768,1024]{1,0:T(8,128)(2,1)}, bf16[768,1024]{1,0:T(8,128)(2,1)S(1)}, u32[]{:S(2)}, u32[]{:S(2)}) collective-permute-start(bf16[768,1024]{1,0:T(8,128)(2,1)} %own.1), channel_id=1, source_target_pairs={{0,1},{1,0},{2,3},{3,2},{4,5},{5,4},{6,7},{7,6},{8,9},{9,8},{10,11... | collective-permute-start | bytes 4718600 | tf_op jit(solution)/shard_map/ppermute | solution.py:27
  0.7 0.7 %reshape.26.gain = bf16[2,1024]{1,0:T(2,128)(2,1)S(1)} reshape(bf16[2048]{0:T(1024)(128)(2,1)} %param.13) | data formatting | bytes 8192 | tf_op jit(solution)/shard_map/reshape | solution.py:273
  1.4 0.0 copy-start.10
  1.4 0.7 %copy-done.10 = f32[4,768]{1,0:T(4,128)S(1)} copy-done((f32[4,768]{1,0:T(4,128)S(1)}, f32[4,768]{1,0:T(4,128)}, u32[]{:S(2)}) %copy-start.10) | copy-done | bytes 12312
  2.1 1.1 %shard_map.118 = (f32[2,2,768]{2,1,0:T(2,128)S(1)}, f32[2,768,2]{2,1,0:T(8,128)S(1)}, f32[768,4]{1,0:T(8,128)S(1)}) custom-call(s32[1]{0:T(128)} %bitcast.pair.which, f32[4,768]{1,0:T(4,128)S(1)} %copy-done.10), custom_call_target="tpu_custom_call" | custom-call | flops 201326592 | bytes 503316 | tf_op jit(solution)/shard_map/pallas_call | solution.py:254
  3.2 0.1 compare_select_fusion
  3.3 1.4 %fusion = (f32[768,128]{1,0:T(8,128)S(1)}, f32[768,128]{1,0:T(8,128)S(1)}) fusion(f32[128]{0:T(128)S(1)} %get-tuple-element.31, f32[128]{0:T(128)S(1)} %get-tuple-element.32, f32[768]{0:T(1024)S(1)} %add_convert_fusion.1), kind=kLoop, calls=%fused_computation.2 | loop fusion | flops 196608 | bytes 790528 | tf_op jit(solution)/shard_map/mul | solution.py:246
  4.7 0.0 collective-permute-done.other
  4.8 0.0 copy-start.3
  4.8 1.6 %copy-done.3 = bf16[2048,512]{1,0:T(8,128)(2,1)S(1)} copy-done((bf16[2048,512]{1,0:T(8,128)(2,1)S(1)}, bf16[2048,512]{1,0:T(8,128)(2,1)}, u32[]{:S(2)}) %copy-start.3) | copy-done | bytes 2097176
  6.4 0.0 copy-start.4
  6.4 1.6 %copy-done.4 = bf16[2048,512]{1,0:T(8,128)(2,1)S(1)} copy-done((bf16[2048,512]{1,0:T(8,128)(2,1)S(1)}, bf16[2048,512]{1,0:T(8,128)(2,1)}, u32[]{:S(2)}) %copy-start.4) | copy-done | bytes 2097176
  7.9 0.0 copy-start.9
  7.9 1.4 %copy-done.9 = bf16[768,1024]{1,0:T(8,128)(2,1)S(1)} copy-done((bf16[768,1024]{1,0:T(8,128)(2,1)S(1)}, bf16[768,1024]{1,0:T(8,128)(2,1)}, u32[]{:S(2)}) %copy-start.9) | copy-done | bytes 1572888
  9.4 0.0 copy-start.5
  9.4 0.0 copy-start.6
  9.4 6.2 %shard_map.119 = (bf16[768,2048]{1,0:T(8,128)(2,1)S(1)}, bf16[768,512]{1,0:T(8,128)(2,1)S(1)}, bf16[768,512]{1,0:T(8,128)(2,1)S(1)}, bf16[4,3,128,128]{3,2,1,0:T(8,128)(2,1)S(1)}, bf16[144,512]{1,0:T(8,128)(2,1)S(1)}) custom-call(s32[1]{0:T(128)} %bitcast.pair.which, bf16[768,1024]{1,0:T(8,128)(2,1)S(1)} %copy-done.9, ...), custom_call_target="tpu_custom_call" | custom-call | flops 3221225472 | bytes 8053063 | tf_op jit(solution)/shard_map/pallas_call | solution.py:263
  15.6 0.0 copy-done.5
  15.6 0.0 copy-done.6
  15.6 0.0 copy-start.7
  15.6 0.0 copy-start.8
  15.6 4.1 %shard_map.122 = (bf16[768,512]{1,0:T(8,128)(2,1)S(1)}, bf16[160,512]{1,0:T(8,128)(2,1)S(1)}) custom-call(s32[1]{0:T(128)} %bitcast.pair.which, bf16[768,2048]{1,0:T(8,128)(2,1)S(1)} %get-tuple-element.18.normed, bf16[2048,512]{1,0:T(8,128)(2,1)S(1)} %copy-done.5, bf16[2048,512]{1,0:T(8,128)(2,1)S(1)} %copy-done.6, bf16[144,512]{1,0:T(8,128)(2,1)S(1)} %get-tuple-element.25.total), custom_call_target="tpu_custom_call" | custom-call | flops 3221225472 | bytes 8053063 | tf_op jit(solution)/shard_map/pallas_call | solution.py:276
  19.7 1.3 %collective-permute-start.1 = (bf16[160,512]{1,0:T(8,128)(2,1)S(1)}, bf16[160,512]{1,0:T(8,128)(2,1)S(1)}, u32[]{:S(2)}, u32[]{:S(2)}) collective-permute-start(bf16[160,512]{1,0:T(8,128)(2,1)S(1)} %get-tuple-element.28), channel_id=1, source_target_pairs={{0,8},{8,16},{16,24},{1,9},{9,17},{17,25},{2,10},{10,18},{18,26},{... | collective-permute-start | bytes 491528 | tf_op jit(solution)/shard_map/ppermute | solution.py:23
  21.0 0.0 copy-done.7
  21.0 0.0 copy-done.8
  21.0 4.2 %shard_map.120 = (bf16[768,512]{1,0:T(8,128)(2,1)S(1)}, bf16[768,512]{1,0:T(8,128)(2,1)S(1)}) custom-call(s32[1]{0:T(128)} %bitcast.pair.which, bf16[768,2048]{1,0:T(8,128)(2,1)S(1)} %get-tuple-element.18.normed, bf16[2048,512]{1,0:T(8,128)(2,1)S(1)} %copy-done.7, bf16[2048,512]{1,0:T(8,128)(2,1)S(1)} %copy-done.8, ...), custom_call_target="tpu_custom_call" | custom-call | flops 3221225472 | bytes 8053063 | tf_op jit(solution)/shard_map/pallas_call | solution.py:300
  25.2 2.1 %collective-permute-done.1.rest_0_ = bf16[160,512]{1,0:T(8,128)(2,1)S(1)} collective-permute-done((bf16[160,512]{1,0:T(8,128)(2,1)S(1)}, bf16[160,512]{1,0:T(8,128)(2,1)S(1)}, u32[]{:S(2)}, u32[]{:S(2)}) %collective-permute-start.1) | collective-permute-done | bytes 163872 | tf_op jit(solution)/shard_map/ppermute | solution.py:23
  27.3 0.1 add_convert_fusion
  27.5 1.5 %collective-permute-start.2 = (bf16[144,512]{1,0:T(8,128)(2,1)S(1)}, bf16[144,512]{1,0:T(8,128)(2,1)S(1)}, u32[]{:S(2)}, u32[]{:S(2)}) collective-permute-start(bf16[144,512]{1,0:T(8,128)(2,1)S(1)} %add_convert_fusion), channel_id=1, source_target_pairs={{0,16},{8,24},{1,17},{9,25},{2,18},{10,26},{3,19},{11,27},{4,20},{... | collective-permute-start | bytes 442376 | tf_op jit(solution)/shard_map/ppermute | solution.py:23
  28.9 0.0 copy-start
  28.9 2.3 %shard_map.121.local = f32[768,512]{1,0:T(8,128)S(1)} custom-call(s32[1]{0:T(128)} %bitcast.pair.which, bf16[768,512]{1,0:T(8,128)(2,1)S(1)} %get-tuple-element.19.queries, bf16[768,512]{1,0:T(8,128)(2,1)S(1)} %get-tuple-element.20.keys, bf16[768,512]{1,0:T(8,128)(2,1)S(1)} %get-tuple-element.21.values, ...), custom_call_target="tpu_custom_call" | custom-call | flops 3221225472 | bytes 8053063 | tf_op jit(solution)/shard_map/pallas_call | solution.py:309
  31.3 7.8 %collective-permute-done.2.rest_1_ = bf16[144,512]{1,0:T(8,128)(2,1)S(1)} collective-permute-done((bf16[144,512]{1,0:T(8,128)(2,1)S(1)}, bf16[144,512]{1,0:T(8,128)(2,1)S(1)}, u32[]{:S(2)}, u32[]{:S(2)}) %collective-permute-start.2) | collective-permute-done | bytes 147488 | tf_op jit(solution)/shard_map/ppermute | solution.py:23
  39.1 0.0 copy-done
  39.1 0.0 copy-start.2
  39.1 1.2 %shard_map.124 = bf16[384,1024]{1,0:T(8,128)(2,1)S(1)} custom-call(s32[1]{0:T(128)} %bitcast.2.which, bf16[768,512]{1,0:T(8,128)(2,1)S(1)} %get-tuple-element.19.queries, f32[768,512]{1,0:T(8,128)S(1)} %shard_map.121.local, f32[768,4]{1,0:T(8,128)S(1)} %get-tuple-element.24.reach, bf16[768,512]{1,0:T(8,128)(2,1)S(1)} %get-tuple-element.26.gated.before, ...), custom_call_target="tpu_custom_call" | custom-call | flops 536870912 | bytes 1342177 | tf_op jit(solution)/shard_map/pallas_call | solution.py:324
  40.3 0.0 copy-start.1
  40.3 0.6 %collective-permute-start.3 = (bf16[384,1024]{1,0:T(8,128)(2,1)S(1)}, bf16[384,1024]{1,0:T(8,128)(2,1)S(1)}, u32[]{:S(2)}, u32[]{:S(2)}) collective-permute-start(bf16[384,1024]{1,0:T(8,128)(2,1)S(1)} %shard_map.124), channel_id=1, source_target_pairs={{0,1},{1,0},{2,3},{3,2},{4,5},{5,4},{6,7},{7,6},{8,9},{9,8},{10,11... | collective-permute-start | bytes 2359304 | tf_op jit(solution)/shard_map/ppermute | solution.py:27
  40.8 1.2 %shard_map.123.kept = bf16[384,1024]{1,0:T(8,128)(2,1)S(1)} custom-call(s32[1]{0:T(128)} %bitcast.pair.which, bf16[768,512]{1,0:T(8,128)(2,1)S(1)} %get-tuple-element.19.queries, f32[768,512]{1,0:T(8,128)S(1)} %shard_map.121.local, f32[768,4]{1,0:T(8,128)S(1)} %get-tuple-element.24.reach, bf16[768,512]{1,0:T(8,128)(2,1)S(1)} %get-tuple-element.26.gated.before, ...), custom_call_target="tpu_custom_call" | custom-call | flops 536870912 | bytes 1342177 | tf_op jit(solution)/shard_map/pallas_call | solution.py:324
  42.0 0.7 %collective-permute-done.3.arrived = bf16[384,1024]{1,0:T(8,128)(2,1)S(1)} collective-permute-done((bf16[384,1024]{1,0:T(8,128)(2,1)S(1)}, bf16[384,1024]{1,0:T(8,128)(2,1)S(1)}, u32[]{:S(2)}, u32[]{:S(2)}) %collective-permute-start.3) | collective-permute-done | bytes 786464 | tf_op jit(solution)/shard_map/ppermute | solution.py:27
  42.7 0.0 copy-done.2
  42.7 0.0 copy-done.1
  42.8 5.4 %shard_map.125 = bf16[384,2048]{1,0:T(8,128)(2,1)} custom-call(s32[1]{0:T(128)} %bitcast.pair.which, bf16[384,1024]{1,0:T(8,128)(2,1)S(1)} %shard_map.123.kept, bf16[384,1024]{1,0:T(8,128)(2,1)S(1)} %collective-permute-done.3.arrived, bf16[1024,2048]{1,0:T(8,128)(2,1)S(1)} %copy-done.1, bf16[1024,2048]{1,0:T(8,128)(2,1)S(1)} %copy-done.2), custom_call_target="tpu_custom_call" | custom-call | flops 3221225472 | bytes 8053063 | tf_op jit(solution)/shard_map/pallas_call | solution.py:345
  (4 shorter events, 0.0 us)
Async XLA Ops:
  0.0 4.7 %collective-permute-start = (bf16[768,1024]{1,0:T(8,128)(2,1)}, bf16[768,1024]{1,0:T(8,128)(2,1)S(1)}, u32[]{:S(2)}, u32[]{:S(2)}) collective-permute-start(bf16[768,1024]{1,0:T(8,128)(2,1)} %own.1), channel_id=1, source_target_pairs={{0,1},{1,0},{2,3},{3,2},{4,5},{5,4},{6,7},{7,6},{8,9},{9,8},{10,11... | collective-permute-start | bytes 4718600 | tf_op jit(solution)/shard_map/ppermute | solution.py:27
  1.4 0.7 %copy-start.10 = (f32[4,768]{1,0:T(4,128)S(1)}, f32[4,768]{1,0:T(4,128)}, u32[]{:S(2)}) copy-start(f32[4,768]{1,0:T(4,128)} %log_decay.1) | copy-start | bytes 36868
  4.8 1.6 %copy-start.3 = (bf16[2048,512]{1,0:T(8,128)(2,1)S(1)}, bf16[2048,512]{1,0:T(8,128)(2,1)}, u32[]{:S(2)}) copy-start(bf16[2048,512]{1,0:T(8,128)(2,1)} %w_key.1) | copy-start | bytes 6291460
  6.4 1.6 %copy-start.4 = (bf16[2048,512]{1,0:T(8,128)(2,1)S(1)}, bf16[2048,512]{1,0:T(8,128)(2,1)}, u32[]{:S(2)}) copy-start(bf16[2048,512]{1,0:T(8,128)(2,1)} %w_value.1) | copy-start | bytes 6291460
  7.9 1.4 %copy-start.9 = (bf16[768,1024]{1,0:T(8,128)(2,1)S(1)}, bf16[768,1024]{1,0:T(8,128)(2,1)}, u32[]{:S(2)}) copy-start(bf16[768,1024]{1,0:T(8,128)(2,1)} %own.1) | copy-start | bytes 4718596
  9.4 6.2 %copy-start.5 = (bf16[2048,512]{1,0:T(8,128)(2,1)S(1)}, bf16[2048,512]{1,0:T(8,128)(2,1)}, u32[]{:S(2)}) copy-start(bf16[2048,512]{1,0:T(8,128)(2,1)} %w_in.1) | copy-start | bytes 6291460
  9.4 6.2 %copy-start.6 = (bf16[2048,512]{1,0:T(8,128)(2,1)S(1)}, bf16[2048,512]{1,0:T(8,128)(2,1)}, u32[]{:S(2)}) copy-start(bf16[2048,512]{1,0:T(8,128)(2,1)} %w_pre.1) | copy-start | bytes 6291460
  15.6 5.4 %copy-start.7 = (bf16[2048,512]{1,0:T(8,128)(2,1)S(1)}, bf16[2048,512]{1,0:T(8,128)(2,1)}, u32[]{:S(2)}) copy-start(bf16[2048,512]{1,0:T(8,128)(2,1)} %w_query.1) | copy-start | bytes 6291460
  15.6 5.4 %copy-start.8 = (bf16[2048,512]{1,0:T(8,128)(2,1)S(1)}, bf16[2048,512]{1,0:T(8,128)(2,1)}, u32[]{:S(2)}) copy-start(bf16[2048,512]{1,0:T(8,128)(2,1)} %w_post.1) | copy-start | bytes 6291460
  19.7 7.6 %collective-permute-start.1 = (bf16[160,512]{1,0:T(8,128)(2,1)S(1)}, bf16[160,512]{1,0:T(8,128)(2,1)S(1)}, u32[]{:S(2)}, u32[]{:S(2)}) collective-permute-start(bf16[160,512]{1,0:T(8,128)(2,1)S(1)} %get-tuple-element.28), channel_id=1, source_target_pairs={{0,8},{8,16},{16,24},{1,9},{9,17},{17,25},{2,10},{10,18},{18,26},{... | collective-permute-start | bytes 491528 | tf_op jit(solution)/shard_map/ppermute | solution.py:23
  27.5 11.6 %collective-permute-start.2 = (bf16[144,512]{1,0:T(8,128)(2,1)S(1)}, bf16[144,512]{1,0:T(8,128)(2,1)S(1)}, u32[]{:S(2)}, u32[]{:S(2)}) collective-permute-start(bf16[144,512]{1,0:T(8,128)(2,1)S(1)} %add_convert_fusion), channel_id=1, source_target_pairs={{0,16},{8,24},{1,17},{9,25},{2,18},{10,26},{3,19},{11,27},{4,20},{... | collective-permute-start | bytes 442376 | tf_op jit(solution)/shard_map/ppermute | solution.py:23
  28.9 10.1 %copy-start = (bf16[3,512]{1,0:T(4,128)(2,1)S(1)}, bf16[3,512]{1,0:T(4,128)(2,1)}, u32[]{:S(2)}) copy-start(bf16[3,512]{1,0:T(4,128)(2,1)} %taps.3) | copy-start | bytes 9220
  39.1 3.7 %copy-start.2 = (bf16[1024,2048]{1,0:T(8,128)(2,1)S(1)}, bf16[1024,2048]{1,0:T(8,128)(2,1)}, u32[]{:S(2)}) copy-start(bf16[1024,2048]{1,0:T(8,128)(2,1)} %w_conv.1) | copy-start | bytes 12582916
  40.3 2.5 %copy-start.1 = (bf16[1024,2048]{1,0:T(8,128)(2,1)S(1)}, bf16[1024,2048]{1,0:T(8,128)(2,1)}, u32[]{:S(2)}) copy-start(bf16[1024,2048]{1,0:T(8,128)(2,1)} %w_ret.1) | copy-start | bytes 12582916
  40.3 2.5 %collective-permute-start.3 = (bf16[384,1024]{1,0:T(8,128)(2,1)S(1)}, bf16[384,1024]{1,0:T(8,128)(2,1)S(1)}, u32[]{:S(2)}, u32[]{:S(2)}) collective-permute-start(bf16[384,1024]{1,0:T(8,128)(2,1)S(1)} %shard_map.124), channel_id=1, source_target_pairs={{0,1},{1,0},{2,3},{3,2},{4,5},{5,4},{6,7},{7,6},{8,9},{9,8},{10,11... | collective-permute-start | bytes 2359304 | tf_op jit(solution)/shard_map/ppermute | solution.py:27

commit v3 on v2

--- a/solution.py
+++ b/solution.py
@@ -29,6 +29,10 @@
 
 def turn(vectors, cosines, sines):
     return vectors * cosines + pltpu.roll(vectors, DH // 2, 1) * sines
+
+
+def held(value):
+    return pltpu.with_memory_space_constraint(value, pltpu.HBM)
 
 
 def contract(left, right, dims):
@@ -84,14 +88,32 @@
         prefix = prefix + column[chunk - 1 : chunk, :]
 
 
-def key_value_kernel(chunk, pair, own, other, gain, w_key, w_value, cosines, sines, cum_col,
-                     normed, keys, values, starts, total):
+def key_value_kernel(chunk, pair, own_far, other, gain, key_far, value_far, cosines, sines,
+                     cum_col, normed, keys, values, starts, total, own, key_near, value_near,
+                     arrivals):
     step = pl.program_id(0)
     rows = normed.shape[0]
     half = own.shape[1]
+    steps = key_near.shape[0]
+    size = key_near.shape[2]
+
+    def fetches(index):
+        lanes = pl.ds(index * size, size)
+        return (
+            pltpu.make_async_copy(key_far.at[:, lanes], key_near.at[index], arrivals.at[0, index]),
+            pltpu.make_async_copy(
+                value_far.at[:, lanes], value_near.at[index], arrivals.at[1, index]
+            ),
+        )
 
     @pl.when(step == 0)
     def _():
+        fetch_own = pltpu.make_async_copy(own_far, own, arrivals.at[2, 0])
+        fetch_own.start()
+        for index in range(steps):
+            for fetch in fetches(index):
+                fetch.start()
+        fetch_own.wait()
         low_gain = gain[0:1, :].astype(F32)
         high_gain = gain[1:2, :].astype(F32)
         my_gain = jnp.where(pair[0] == 0, low_gain, high_gain)
@@ -105,10 +127,17 @@
             normed[rng, :half] = (mine * scale * my_gain).astype(BF16)
             normed[rng, half:] = (theirs * scale * their_gain).astype(BF16)
 
-    projected_keys = project(pair, normed, w_key)
-    projected_values = project(pair, normed, w_value)
+    for index in range(steps):
+
+        @pl.when(step == index)
+        def _(index=index):
+            for fetch in fetches(index):
+                fetch.wait()
+
+    projected_keys = project(pair, normed, key_near.at[step])
+    projected_values = project(pair, normed, value_near.at[step])
     values[...] = projected_values.astype(BF16)
-    for head in range(w_key.shape[1] // DH):
+    for head in range(size // DH):
         lanes = slice(head * DH, (head + 1) * DH)
         turned = turn(projected_keys[:, lanes], cosines[...], sines[...]) * DH ** (-0.5)
         turned = turned.astype(BF16)
@@ -198,13 +227,15 @@
 
 def output_kernel(pair, kept, arrived, w_ret, w_conv, mixed):
     width = w_ret.shape[0] // 2
-    mine = pl.multiple_of(pair[0] * width, width)
-    theirs = pl.multiple_of((1 - pair[0]) * width, width)
+    tile = mixed.shape[1]
+    lanes = pl.ds(pl.multiple_of(pl.program_id(0) * tile, tile), tile)
+    mine = pl.ds(pl.multiple_of(pair[0] * width, width), width)
+    theirs = pl.ds(pl.multiple_of((1 - pair[0]) * width, width), width)
     mixed[...] = (
-        jnp.dot(kept[:, :width], w_ret[pl.ds(mine, width), :], preferred_element_type=F32)
-        + jnp.dot(kept[:, width:], w_conv[pl.ds(mine, width), :], preferred_element_type=F32)
-        + jnp.dot(arrived[:, :width], w_ret[pl.ds(theirs, width), :], preferred_element_type=F32)
-        + jnp.dot(arrived[:, width:], w_conv[pl.ds(theirs, width), :], preferred_element_type=F32)
+        jnp.dot(kept[:, :width], w_ret[mine, lanes], preferred_element_type=F32)
+        + jnp.dot(kept[:, width:], w_conv[mine, lanes], preferred_element_type=F32)
+        + jnp.dot(arrived[:, :width], w_ret[theirs, lanes], preferred_element_type=F32)
+        + jnp.dot(arrived[:, width:], w_conv[theirs, lanes], preferred_element_type=F32)
     ).astype(BF16)
 
 
@@ -248,6 +279,8 @@
     full = lambda *shape: pl.BlockSpec(shape, lambda j, s: (0,) * len(shape))
     columns = lambda height, size: pl.BlockSpec((height, size), lambda j, s: (0, j))
     lead = lambda *shape: pl.BlockSpec(shape, lambda j, s: (j,) + (0,) * (len(shape) - 1))
+    far = pl.BlockSpec(memory_space=pltpu.HBM)
+    near = pl.BlockSpec(memory_space=pltpu.VMEM)
     arr = jax.ShapeDtypeStruct
     unit = 2 * rows * depth * width
 
@@ -263,15 +296,17 @@
     normed, keys, values, starts, total = call(
         functools.partial(key_value_kernel, chunk),
         (steps,),
-        [full(rows, half), full(rows, half), full(2, half), columns(depth, gw), columns(depth, gw),
+        [far, full(rows, half), full(2, half), far, far,
          full(rows, DH), full(rows, DH), lead(1, rows, group)],
         [full(rows, depth), columns(rows, gw), columns(rows, gw),
          lead(group, chunks, DH, DH), columns(DH + PACK, gw)],
         [arr((rows, depth), BF16), arr((rows, width), BF16), arr((rows, width), BF16),
          arr((heads, chunks, DH, DH), BF16), arr((DH + PACK, width), BF16)],
         2 * unit,
-    )(pair_scalar, tokens, other, norm_gain.reshape(2, half), w_key, w_value, cosines, sines,
-      cum_col)
+        [pltpu.VMEM((rows, half), BF16), pltpu.VMEM((steps, depth, gw), BF16),
+         pltpu.VMEM((steps, depth, gw), BF16), pltpu.SemaphoreType.DMA((3, steps))],
+    )(pair_scalar, held(tokens), other, norm_gain.reshape(2, half), held(w_key), held(w_value),
+      cosines, sines, cum_col)
 
     gated, window = call(
         gate_kernel,
@@ -346,7 +381,7 @@
         output_kernel,
         (model // tile,),
         [full(part, merged_width), full(part, merged_width),
-         columns(w_out_ret.shape[0], tile), columns(w_out_conv.shape[0], tile)],
+         near, near],
         columns(part, tile),
         arr((part, model), BF16),
         2 * unit,

time: 48.6 us -> 44.5 us (0.916)
  local copies, waits for them, and re-layouts: 6.05 us -> 1.49 us
  Pallas kernels: 25.7 us -> 26.2 us
    unnamed x22 -> x16, local copies, waits for them, and re-layouts: 5.35 us -> 0.79 us
    pallas_call x1, Pallas kernels: 6.21 us -> 7.53 us  [body(): call(functools.partial(key_value_kernel, chunk), (steps,), [far, full(row...]
    pallas_call x1, Pallas kernels: 5.44 us -> 4.76 us  [body(): call(output_kernel, (model // tile,), [full(part, merged_width), full(par...]
  transfers between devices with their start and end apart: 4 -> 4, of which waited for: 3 -> 3; matrix products, arithmetic and copies ran while one was open for 5% -> 5% of each run, Pallas kernels for 18% -> 20%
where the time goes in v3:
time: 44.5 us; the launch traced here: 44.3 us
  Pallas kernels  26.2 us (59%)
  waiting for transfers between devices  10.7 us (24%)
  starting transfers between devices  4 us (9%)
  other arithmetic  1.66 us (4%)
  local copies, waits for them, and re-layouts  1.49 us (3%)
    ppermute x2, waiting for transfers between devices, shifted(): lax.ppermute(value, axis, [(source, source + steps) for source in range(f...  9.95 us
    pallas_call x1, Pallas kernels, body(): call(functools.partial(key_value_kernel, chunk), (steps,), [far, full(row...  7.53 us
    pallas_call x1, Pallas kernels, body(): call(output_kernel, (model // tile,), [full(part, merged_width), full(par...  4.76 us
    pallas_call x1, Pallas kernels, body(): call(query_kernel, (steps,), [full(rows, depth), columns(depth, gw), colu...  4.19 us
    pallas_call x1, Pallas kernels, body(): call(gate_kernel, (steps,), [full(rows, depth), columns(depth, cgw), colu...  4.02 us
    ppermute x2, starting transfers between devices, shifted(): lax.ppermute(value, axis, [(source, source + steps) for source in range(f...  2.76 us
    pallas_call x2, Pallas kernels, finish(): call(functools.partial(finish_kernel, len(received)), (1,), [piece(width)...  2.31 us
    pallas_call x1, Pallas kernels, body(): call(functools.partial(local_kernel, chunk), (steps,), [columns(rows, gw)...  2.3 us
  transfers between devices with their start and end apart: 4, of which 3 were waited for; matrix products, arithmetic and copies ran while one was open for 5% of the time, Pallas kernels for 20%

profile of v3, /device:TPU:29, one launch (start us, length us, event | category | flops | bytes accessed | tf_op | source)
XLA Modules:
  0.0 44.3 jit_solution(11320063226785253000)
XLA Ops:
  0.0 0.7 %collective-permute-start = (bf16[768,1024]{1,0:T(8,128)(2,1)}, bf16[768,1024]{1,0:T(8,128)(2,1)S(1)}, u32[]{:S(2)}, u32[]{:S(2)}) collective-permute-start(bf16[768,1024]{1,0:T(8,128)(2,1)} %own_far.1), channel_id=1, source_target_pairs={{0,1},{1,0},{2,3},{3,2},{4,5},{5,4},{6,7},{7,6},{8,9},{9,8},{10,11... | collective-permute-start | bytes 4718600 | tf_op jit(solution)/shard_map/ppermute | solution.py:27
  0.7 0.7 %reshape.26.gain = bf16[2,1024]{1,0:T(2,128)(2,1)S(1)} reshape(bf16[2048]{0:T(1024)(128)(2,1)} %param.13) | data formatting | bytes 8192 | tf_op jit(solution)/shard_map/reshape | solution.py:308
  1.4 0.0 copy-start.7
  1.4 0.7 %copy-done.7 = f32[4,768]{1,0:T(4,128)S(1)} copy-done((f32[4,768]{1,0:T(4,128)S(1)}, f32[4,768]{1,0:T(4,128)}, u32[]{:S(2)}) %copy-start.7) | copy-done | bytes 12312
  2.1 1.1 %shard_map.118 = (f32[2,2,768]{2,1,0:T(2,128)S(1)}, f32[2,768,2]{2,1,0:T(8,128)S(1)}, f32[768,4]{1,0:T(8,128)S(1)}) custom-call(s32[1]{0:T(128)} %bitcast.pair.which, f32[4,768]{1,0:T(4,128)S(1)} %copy-done.7), custom_call_target="tpu_custom_call" | custom-call | flops 201326592 | bytes 503316 | tf_op jit(solution)/shard_map/pallas_call | solution.py:287
  3.2 0.1 compare_select_fusion
  3.3 1.4 %fusion = (f32[768,128]{1,0:T(8,128)S(1)}, f32[768,128]{1,0:T(8,128)S(1)}) fusion(f32[128]{0:T(128)S(1)} %get-tuple-element.31, f32[128]{0:T(128)S(1)} %get-tuple-element.32, f32[768]{0:T(1024)S(1)} %add_convert_fusion.1), kind=kLoop, calls=%fused_computation.2 | loop fusion | flops 196608 | bytes 790528 | tf_op jit(solution)/shard_map/mul | solution.py:277
  4.7 0.0 collective-permute-done.other
  4.8 0.0 copy-start.3
  4.8 0.0 copy-start.4
  4.8 7.5 %shard_map.119 = (bf16[768,2048]{1,0:T(8,128)(2,1)S(1)}, bf16[768,512]{1,0:T(8,128)(2,1)S(1)}, bf16[768,512]{1,0:T(8,128)(2,1)S(1)}, bf16[4,3,128,128]{3,2,1,0:T(8,128)(2,1)S(1)}, bf16[144,512]{1,0:T(8,128)(2,1)S(1)}) custom-call(s32[1]{0:T(128)} %bitcast.pair.which, bf16[768,1024]{1,0:T(8,128)(2,1)} %own_far.1, ...), custom_call_target="tpu_custom_call" | custom-call | flops 3221225472 | bytes 8053063 | tf_op jit(solution)/shard_map/pallas_call | solution.py:296
  12.3 0.0 copy-done.3
  12.3 0.0 copy-done.4
  12.3 0.0 copy-start.5
  12.4 0.0 copy-start.6
  12.4 4.0 %shard_map.122 = (bf16[768,512]{1,0:T(8,128)(2,1)S(1)}, bf16[160,512]{1,0:T(8,128)(2,1)S(1)}) custom-call(s32[1]{0:T(128)} %bitcast.pair.which, bf16[768,2048]{1,0:T(8,128)(2,1)S(1)} %get-tuple-element.18.normed, bf16[2048,512]{1,0:T(8,128)(2,1)S(1)} %copy-done.3, bf16[2048,512]{1,0:T(8,128)(2,1)S(1)} %copy-done.4, bf16[144,512]{1,0:T(8,128)(2,1)S(1)} %get-tuple-element.25.total), custom_call_target="tpu_custom_call" | custom-call | flops 3221225472 | bytes 8053063 | tf_op jit(solution)/shard_map/pallas_call | solution.py:311
  16.4 1.3 %collective-permute-start.1 = (bf16[160,512]{1,0:T(8,128)(2,1)S(1)}, bf16[160,512]{1,0:T(8,128)(2,1)S(1)}, u32[]{:S(2)}, u32[]{:S(2)}) collective-permute-start(bf16[160,512]{1,0:T(8,128)(2,1)S(1)} %get-tuple-element.28), channel_id=1, source_target_pairs={{0,8},{8,16},{16,24},{1,9},{9,17},{17,25},{2,10},{10,18},{18,26},{... | collective-permute-start | bytes 491528 | tf_op jit(solution)/shard_map/ppermute | solution.py:23
  17.7 0.0 copy-done.5
  17.7 0.0 copy-done.6
  17.7 4.2 %shard_map.120 = (bf16[768,512]{1,0:T(8,128)(2,1)S(1)}, bf16[768,512]{1,0:T(8,128)(2,1)S(1)}) custom-call(s32[1]{0:T(128)} %bitcast.pair.which, bf16[768,2048]{1,0:T(8,128)(2,1)S(1)} %get-tuple-element.18.normed, bf16[2048,512]{1,0:T(8,128)(2,1)S(1)} %copy-done.5, bf16[2048,512]{1,0:T(8,128)(2,1)S(1)} %copy-done.6, ...), custom_call_target="tpu_custom_call" | custom-call | flops 3221225472 | bytes 8053063 | tf_op jit(solution)/shard_map/pallas_call | solution.py:335
  21.9 2.1 %collective-permute-done.1.rest_0_ = bf16[160,512]{1,0:T(8,128)(2,1)S(1)} collective-permute-done((bf16[160,512]{1,0:T(8,128)(2,1)S(1)}, bf16[160,512]{1,0:T(8,128)(2,1)S(1)}, u32[]{:S(2)}, u32[]{:S(2)}) %collective-permute-start.1) | collective-permute-done | bytes 163872 | tf_op jit(solution)/shard_map/ppermute | solution.py:23
  24.0 0.1 add_convert_fusion
  24.1 1.5 %collective-permute-start.2 = (bf16[144,512]{1,0:T(8,128)(2,1)S(1)}, bf16[144,512]{1,0:T(8,128)(2,1)S(1)}, u32[]{:S(2)}, u32[]{:S(2)}) collective-permute-start(bf16[144,512]{1,0:T(8,128)(2,1)S(1)} %add_convert_fusion), channel_id=1, source_target_pairs={{0,16},{8,24},{1,17},{9,25},{2,18},{10,26},{3,19},{11,27},{4,20},{... | collective-permute-start | bytes 442376 | tf_op jit(solution)/shard_map/ppermute | solution.py:23
  25.6 0.0 copy-start
  25.6 2.3 %shard_map.121.local = f32[768,512]{1,0:T(8,128)S(1)} custom-call(s32[1]{0:T(128)} %bitcast.pair.which, bf16[768,512]{1,0:T(8,128)(2,1)S(1)} %get-tuple-element.19.queries, bf16[768,512]{1,0:T(8,128)(2,1)S(1)} %get-tuple-element.20.keys, bf16[768,512]{1,0:T(8,128)(2,1)S(1)} %get-tuple-element.21.values, ...), custom_call_target="tpu_custom_call" | custom-call | flops 3221225472 | bytes 8053063 | tf_op jit(solution)/shard_map/pallas_call | solution.py:344
  28.0 7.8 %collective-permute-done.2.rest_1_ = bf16[144,512]{1,0:T(8,128)(2,1)S(1)} collective-permute-done((bf16[144,512]{1,0:T(8,128)(2,1)S(1)}, bf16[144,512]{1,0:T(8,128)(2,1)S(1)}, u32[]{:S(2)}, u32[]{:S(2)}) %collective-permute-start.2) | collective-permute-done | bytes 147488 | tf_op jit(solution)/shard_map/ppermute | solution.py:23
  35.8 0.0 copy-done
  35.8 0.0 copy-start.2
  35.8 1.2 %shard_map.124 = bf16[384,1024]{1,0:T(8,128)(2,1)S(1)} custom-call(s32[1]{0:T(128)} %bitcast.2.which, bf16[768,512]{1,0:T(8,128)(2,1)S(1)} %get-tuple-element.19.queries, f32[768,512]{1,0:T(8,128)S(1)} %shard_map.121.local, f32[768,4]{1,0:T(8,128)S(1)} %get-tuple-element.24.reach, bf16[768,512]{1,0:T(8,128)(2,1)S(1)} %get-tuple-element.26.gated.before, ...), custom_call_target="tpu_custom_call" | custom-call | flops 536870912 | bytes 1342177 | tf_op jit(solution)/shard_map/pallas_call | solution.py:359
  37.0 0.0 copy-start.1
  37.0 0.6 %collective-permute-start.3 = (bf16[384,1024]{1,0:T(8,128)(2,1)S(1)}, bf16[384,1024]{1,0:T(8,128)(2,1)S(1)}, u32[]{:S(2)}, u32[]{:S(2)}) collective-permute-start(bf16[384,1024]{1,0:T(8,128)(2,1)S(1)} %shard_map.124), channel_id=1, source_target_pairs={{0,1},{1,0},{2,3},{3,2},{4,5},{5,4},{6,7},{7,6},{8,9},{9,8},{10,11... | collective-permute-start | bytes 2359304 | tf_op jit(solution)/shard_map/ppermute | solution.py:27
  37.5 1.2 %shard_map.123.kept = bf16[384,1024]{1,0:T(8,128)(2,1)S(1)} custom-call(s32[1]{0:T(128)} %bitcast.pair.which, bf16[768,512]{1,0:T(8,128)(2,1)S(1)} %get-tuple-element.19.queries, f32[768,512]{1,0:T(8,128)S(1)} %shard_map.121.local, f32[768,4]{1,0:T(8,128)S(1)} %get-tuple-element.24.reach, bf16[768,512]{1,0:T(8,128)(2,1)S(1)} %get-tuple-element.26.gated.before, ...), custom_call_target="tpu_custom_call" | custom-call | flops 536870912 | bytes 1342177 | tf_op jit(solution)/shard_map/pallas_call | solution.py:359
  38.7 0.8 %collective-permute-done.3.arrived = bf16[384,1024]{1,0:T(8,128)(2,1)S(1)} collective-permute-done((bf16[384,1024]{1,0:T(8,128)(2,1)S(1)}, bf16[384,1024]{1,0:T(8,128)(2,1)S(1)}, u32[]{:S(2)}, u32[]{:S(2)}) %collective-permute-start.3) | collective-permute-done | bytes 786464 | tf_op jit(solution)/shard_map/ppermute | solution.py:27
  39.4 0.0 copy-done.2
  39.4 0.0 copy-done.1
  39.5 4.8 %shard_map.125 = bf16[384,2048]{1,0:T(8,128)(2,1)} custom-call(s32[1]{0:T(128)} %bitcast.pair.which, bf16[384,1024]{1,0:T(8,128)(2,1)S(1)} %shard_map.123.kept, bf16[384,1024]{1,0:T(8,128)(2,1)S(1)} %collective-permute-done.3.arrived, bf16[1024,2048]{1,0:T(8,128)(2,1)S(1)} %copy-done.1, bf16[1024,2048]{1,0:T(8,128)(2,1)S(1)} %copy-done.2), custom_call_target="tpu_custom_call" | custom-call | flops 3221225472 | bytes 8053063 | tf_op jit(solution)/shard_map/pallas_call | solution.py:380
  (4 shorter events, 0.0 us)
Async XLA Ops:
  0.0 4.7 %collective-permute-start = (bf16[768,1024]{1,0:T(8,128)(2,1)}, bf16[768,1024]{1,0:T(8,128)(2,1)S(1)}, u32[]{:S(2)}, u32[]{:S(2)}) collective-permute-start(bf16[768,1024]{1,0:T(8,128)(2,1)} %own_far.1), channel_id=1, source_target_pairs={{0,1},{1,0},{2,3},{3,2},{4,5},{5,4},{6,7},{7,6},{8,9},{9,8},{10,11... | collective-permute-start | bytes 4718600 | tf_op jit(solution)/shard_map/ppermute | solution.py:27
  1.4 0.7 %copy-start.7 = (f32[4,768]{1,0:T(4,128)S(1)}, f32[4,768]{1,0:T(4,128)}, u32[]{:S(2)}) copy-start(f32[4,768]{1,0:T(4,128)} %log_decay.1) | copy-start | bytes 36868
  4.8 7.6 %copy-start.3 = (bf16[2048,512]{1,0:T(8,128)(2,1)S(1)}, bf16[2048,512]{1,0:T(8,128)(2,1)}, u32[]{:S(2)}) copy-start(bf16[2048,512]{1,0:T(8,128)(2,1)} %w_in.1) | copy-start | bytes 6291460
  4.8 7.6 %copy-start.4 = (bf16[2048,512]{1,0:T(8,128)(2,1)S(1)}, bf16[2048,512]{1,0:T(8,128)(2,1)}, u32[]{:S(2)}) copy-start(bf16[2048,512]{1,0:T(8,128)(2,1)} %w_pre.1) | copy-start | bytes 6291460
  12.3 5.4 %copy-start.5 = (bf16[2048,512]{1,0:T(8,128)(2,1)S(1)}, bf16[2048,512]{1,0:T(8,128)(2,1)}, u32[]{:S(2)}) copy-start(bf16[2048,512]{1,0:T(8,128)(2,1)} %w_query.1) | copy-start | bytes 6291460
  12.4 5.4 %copy-start.6 = (bf16[2048,512]{1,0:T(8,128)(2,1)S(1)}, bf16[2048,512]{1,0:T(8,128)(2,1)}, u32[]{:S(2)}) copy-start(bf16[2048,512]{1,0:T(8,128)(2,1)} %w_post.1) | copy-start | bytes 6291460
  16.4 7.6 %collective-permute-start.1 = (bf16[160,512]{1,0:T(8,128)(2,1)S(1)}, bf16[160,512]{1,0:T(8,128)(2,1)S(1)}, u32[]{:S(2)}, u32[]{:S(2)}) collective-permute-start(bf16[160,512]{1,0:T(8,128)(2,1)S(1)} %get-tuple-element.28), channel_id=1, source_target_pairs={{0,8},{8,16},{16,24},{1,9},{9,17},{17,25},{2,10},{10,18},{18,26},{... | collective-permute-start | bytes 491528 | tf_op jit(solution)/shard_map/ppermute | solution.py:23
  24.1 11.6 %collective-permute-start.2 = (bf16[144,512]{1,0:T(8,128)(2,1)S(1)}, bf16[144,512]{1,0:T(8,128)(2,1)S(1)}, u32[]{:S(2)}, u32[]{:S(2)}) collective-permute-start(bf16[144,512]{1,0:T(8,128)(2,1)S(1)} %add_convert_fusion), channel_id=1, source_target_pairs={{0,16},{8,24},{1,17},{9,25},{2,18},{10,26},{3,19},{11,27},{4,20},{... | collective-permute-start | bytes 442376 | tf_op jit(solution)/shard_map/ppermute | solution.py:23
  25.6 10.2 %copy-start = (bf16[3,512]{1,0:T(4,128)(2,1)S(1)}, bf16[3,512]{1,0:T(4,128)(2,1)}, u32[]{:S(2)}) copy-start(bf16[3,512]{1,0:T(4,128)(2,1)} %taps.3) | copy-start | bytes 9220
  35.8 3.7 %copy-start.2 = (bf16[1024,2048]{1,0:T(8,128)(2,1)S(1)}, bf16[1024,2048]{1,0:T(8,128)(2,1)}, u32[]{:S(2)}) copy-start(bf16[1024,2048]{1,0:T(8,128)(2,1)} %w_conv.1) | copy-start | bytes 12582916
  37.0 2.5 %copy-start.1 = (bf16[1024,2048]{1,0:T(8,128)(2,1)S(1)}, bf16[1024,2048]{1,0:T(8,128)(2,1)}, u32[]{:S(2)}) copy-start(bf16[1024,2048]{1,0:T(8,128)(2,1)} %w_ret.1) | copy-start | bytes 12582916
  37.0 2.5 %collective-permute-start.3 = (bf16[384,1024]{1,0:T(8,128)(2,1)S(1)}, bf16[384,1024]{1,0:T(8,128)(2,1)S(1)}, u32[]{:S(2)}, u32[]{:S(2)}) collective-permute-start(bf16[384,1024]{1,0:T(8,128)(2,1)S(1)} %shard_map.124), channel_id=1, source_target_pairs={{0,1},{1,0},{2,3},{3,2},{4,5},{5,4},{6,7},{7,6},{8,9},{9,8},{10,11... | collective-permute-start | bytes 2359304 | tf_op jit(solution)/shard_map/ppermute | solution.py:27
